TPU v7x, 512 devices: a whole 4x8x8 slice. The times are simulated.
512 devices in a mesh: sp: 64 (over z, y), tp: 8 (over x, core).
Axes of the slice: x: 4, y: 8, z: 8, core: 2. Of those that a mesh axis runs over, the one named last changes fastest.
Arguments:
- stream: bfloat16 [24576, 2048], P('sp', 'tp'), may hold values from -6 to 6
- norm_gain: float32 [2, 2048], replicated, may hold values from 0.1 to 1.9
- a_weight: bfloat16 [2, 2048, 2048], P(None, 'sp', 'tp'), may hold values from -0.125 to 0.125
- gate_weight: bfloat16 [2, 2048, 2048], P(None, 'sp', 'tp'), may hold values from -0.125 to 0.125
- conv_weight: float32 [2, 31, 2048], P(None, None, 'tp'), may hold values from -4 to 4, as said below
- conv_bias: float32 [2, 2048], P(None, 'tp'), may hold values from -3 to 3
- ln_gain: float32 [2, 2048], P(None, 'tp'), may hold values from 0.1 to 1.9
- ln_shift: float32 [2, 2048], P(None, 'tp'), may hold values from -3 to 3
- out_weight: bfloat16 [2, 2048, 2048], P(None, 'sp', 'tp'), may hold values from -0.125 to 0.125
Outputs:
- result: bfloat16 [24576, 2048], P('sp', 'tp')
Inputs may be any that keep to these rules, and one draw needn't show every extreme that they name: `conv_weight`: each column is drawn with its own scale, and blocks of 16 channels differ in scale by up to a factor of nine.
All inputs are finite; a program needn't handle non-finite values.
Results may differ from a plain program's by a relative error of at most 0.01.
Values may be sent and summed in bfloat16 or wider, within the bound.
A program may use at most 64 MiB of HBM per device.

v0:
```python
import jax
import jax.numpy as jnp
from jax import lax
from jax.sharding import PartitionSpec as P

D = 2048


EPSILON = 1e-06


def in_one_piece(arrays, axis, dim, along):
    ends, at = ([], 0)
    for a in arrays[:-1]:
        at += a.shape[along]
        ends.append(at)
    both = jnp.concatenate(arrays, axis=along)
    return tuple(jnp.split(lax.all_gather(both, axis, axis=dim, tiled=True), ends, axis=along))


def with_halo(block, sides, width):
    for axis, dim in sides:
        count = lax.axis_size(axis)
        forward = [(i, i + 1) for i in range(count - 1)]
        backward = [(target, source) for source, target in forward]
        low = lax.ppermute(
            lax.slice_in_dim(block, block.shape[dim] - width, None, axis=dim), axis, forward
        )
        high = lax.ppermute(lax.slice_in_dim(block, 0, width, axis=dim), axis, backward)
        block = jnp.concatenate([low, block, high], axis=dim)
    return block


def joined_along(pieces, dim):
    pieces = jnp.moveaxis(pieces, 0, dim)
    lengths = pieces.shape
    return pieces.reshape(*lengths[:dim], lengths[dim] * lengths[dim + 1], *lengths[dim + 2 :])


def from_everyone(x, axis):
    length = lax.axis_size(axis)
    return lax.all_to_all(jnp.broadcast_to(x[None], (length, *x.shape)), axis, 0, 0, tiled=True)


def gather_directly(x, axis, dim):
    return joined_along(from_everyone(x, axis), dim)


def taken_together(x, axis):
    return from_everyone(x, axis).sum(axis=0)


def packed_total(arrays, axis):
    line, at, gathered = (jnp.concatenate([a.reshape(-1) for a in arrays]), 0, [])
    so_far = taken_together(line, axis)
    for a in arrays:
        gathered.append(so_far[at : at + a.size].reshape(a.shape))
        at += a.size
    return tuple(gathered)


def normalize_rows(stream_f, gain):
    factor = lax.rsqrt(jnp.mean(stream_f * stream_f, axis=1, keepdims=True) + EPSILON)
    return (stream_f * factor * gain[None, :]).astype(jnp.bfloat16)


def convolve(padded, kernel, conv_shift, out_rows):
    summed = jnp.zeros((out_rows, padded.shape[1]), jnp.float32) + conv_shift[None, :]
    for offset in range(kernel.shape[0]):
        window = lax.slice_in_dim(padded, offset, offset + out_rows, axis=0).astype(jnp.float32)
        summed = summed + window * kernel[offset][None, :]
    return summed


def finish_norm(conv_out, row_sum, row_squares, gain, shift):
    average = row_sum / D
    variance = row_squares / D - average * average
    normed = (conv_out - average) * lax.rsqrt(variance + EPSILON) * gain[None, :] + shift[None, :]
    return jax.nn.silu(normed).astype(jnp.bfloat16)


def local(
    stream, norm_gain, a_weight, gate_weight, conv_weight, conv_bias, ln_gain, ln_shift, out_weight
):
    token_count = stream.shape[0]
    reach = (conv_weight.shape[1] - 1) // 2
    layer_total = a_weight.shape[0]
    sequence_total = token_count * lax.axis_size("sp")
    gathered = in_one_piece((a_weight, gate_weight, out_weight), "sp", 1, 0)
    current = with_halo(stream, (("sp", 0),), layer_total * reach)
    for layer_index in range(layer_total):
        stream_f = current.astype(jnp.float32)
        full_rows = gather_directly(current, "tp", 1)
        normed = normalize_rows(full_rows.astype(jnp.float32), norm_gain[layer_index])
        row_count = normed.shape[0]
        linear = jnp.dot(normed, gathered[0][layer_index], preferred_element_type=jnp.float32)
        gating = jnp.dot(normed, gathered[1][layer_index], preferred_element_type=jnp.float32)
        product = linear * jax.nn.sigmoid(gating)
        margin = (layer_total - layer_index) * reach
        position = (
            lax.axis_index("sp") * token_count - margin + jnp.arange(row_count, dtype=jnp.int32)
        )
        inside = (position >= 0) & (position < sequence_total)
        padded = jnp.where(inside[:, None], product, 0.0).astype(jnp.bfloat16)
        residual = stream_f[reach : row_count - reach]
        out_rows = padded.shape[0] - 2 * reach
        conv_out = convolve(padded, conv_weight[layer_index], conv_bias[layer_index], out_rows)
        row_sum, row_squares = packed_total(
            (
                jnp.sum(conv_out, axis=1, keepdims=True),
                jnp.sum(conv_out * conv_out, axis=1, keepdims=True),
            ),
            "tp",
        )
        mixed_in = finish_norm(
            conv_out, row_sum, row_squares, ln_gain[layer_index], ln_shift[layer_index]
        )
        mixed_rows = gather_directly(mixed_in, "tp", 1)
        branch = jnp.dot(mixed_rows, gathered[2][layer_index], preferred_element_type=jnp.float32)
        current = (residual + branch).astype(jnp.bfloat16)
    return current


def solution(mesh):
    placed = (
        P("sp", "tp"),
        P(),
        P(None, "sp", "tp"),
        P(None, "sp", "tp"),
        P(None, None, "tp"),
        P(None, "tp"),
        P(None, "tp"),
        P(None, "tp"),
        P(None, "sp", "tp"),
    )
    return jax.shard_map(
        local, mesh=mesh, in_specs=placed, out_specs=P("sp", "tp"), check_vma=False
    )
```

profile of v0, /device:TPU:1, one launch (start us, length us, event | category | flops | bytes accessed | tf_op | source)
XLA Modules:
  0.0 229.0 jit_solution(1571828732264705712)
XLA Ops:
  6.5 0.0 all-gather.2.cloned.1.call-start
  6.5 1.4 pad_maximum_fusion.1
  8.0 0.0 all-gather.2.cloned.1.call-update
  8.0 0.7 fusion.28
  8.8 1.3 collective-permute-start.1
  10.0 4.6 %collective-permute-start = (bf16[30,256]{1,0:T(8,128)(2,1)S(1)}, bf16[30,256]{1,0:T(8,128)(2,1)S(1)}, u32[]{:S(2)}, u32[]{:S(2)}) collective-permute-start(bf16[30,256]{1,0:T(8,128)(2,1)S(1)} %get-tuple-element.13), channel_id=1, source_target_pairs={{0,8},{8,16},{16,24},{24,32},{32,40},{40,48},{48,56},{56,64},{64,7... | collective-permute-start | bytes 46088 | tf_op jit(solution)/shard_map/ppermute | solution.py:26
  14.7 0.0 collective-permute-done.1
  14.7 0.8 collective-permute-done
  15.5 1.0 pad_maximum_fusion
  16.5 1.4 broadcast_in_dim.37
  17.9 0.0 copy-start.1
  17.9 0.0 copy-start.2
  17.9 0.0 copy-start.3
  17.9 0.0 copy-start
  17.9 10.9 %all-to-all-start = ((bf16[8,444,256]{2,1,0:T(8,128)(2,1)}), bf16[8,444,256]{2,1,0:T(8,128)(2,1)S(1)}, u32[]{:S(2)}, u32[]{:S(2)}) async-start(bf16[8,444,256]{2,1,0:T(8,128)(2,1)} %broadcast_in_dim.37), calls=%async_computation | async-start | bytes 3670016 | tf_op jit(solution)/shard_map/all_to_all | solution.py:42
  28.8 0.0 copy-done.1
  28.9 0.0 copy-done.2
  28.9 0.0 copy-done.3
  29.0 0.0 copy-done
  29.1 23.2 %all-to-all-done = bf16[8,444,256]{2,1,0:T(8,128)(2,1)S(1)} async-done(((bf16[8,444,256]{2,1,0:T(8,128)(2,1)}), bf16[8,444,256]{2,1,0:T(8,128)(2,1)S(1)}, u32[]{:S(2)}, u32[]{:S(2)}) %all-to-all-start) | async-done | bytes 1818656 | tf_op jit(solution)/shard_map/all_to_all | solution.py:42
  52.3 0.4 fusion
  52.7 0.5 fusion.6
  53.2 1.0 copy.19
  54.3 0.1 pad.10
  54.4 0.6 copy.31
  55.0 50.2 %all-gather.2.cloned.1.call-done = bf16[6,2048,256]{2,1,0:T(8,128)(2,1)} async-done(((bf16[6,32,256]{2,1,0:T(8,128)(2,1)}), bf16[6,2048,256]{2,1,0:T(8,128)(2,1)}) %all-gather.2.cloned.1.call-update) | async-done | bytes 6291472 | tf_op jit(solution)/shard_map/all_gather | solution.py:18
  105.2 1.9 fusion.11
  107.1 1.9 fusion.16
  109.0 0.0 copy-start.4
  109.0 1.9 fusion.26
  110.8 0.1 pad_maximum_fusion.2
  110.9 0.6 broadcast_in_dim.39
  111.5 6.1 %all-to-all-start.1 = ((f32[8,1,828]{2,1,0:T(1,128)}), f32[8,1,828]{2,1,0:T(1,128)S(1)}, u32[]{:S(2)}, u32[]{:S(2)}) async-start(f32[8,1,828]{2,1,0:T(1,128)} %broadcast_in_dim.39), calls=%async_computation.1 | async-start | bytes 57344 | tf_op jit(solution)/shard_map/all_to_all | solution.py:42
  117.7 0.0 copy-done.4
  117.7 4.7 %all-to-all-done.1 = f32[8,1,828]{2,1,0:T(1,128)S(1)} async-done(((f32[8,1,828]{2,1,0:T(1,128)}), f32[8,1,828]{2,1,0:T(1,128)S(1)}, u32[]{:S(2)}, u32[]{:S(2)}) %all-to-all-start.1) | async-done | bytes 26528 | tf_op jit(solution)/shard_map/all_to_all | solution.py:42
  122.4 0.1 slice_multiply_fusion.1
  122.5 0.2 multiply_convert_fusion
  122.7 0.1 broadcast_in_dim.40
  122.8 25.3 %all_to_all.32 = bf16[8,414,256]{2,1,0:T(8,128)(2,1)S(1)} all-to-all(bf16[8,414,256]{2,1,0:T(8,128)(2,1)S(1)} %broadcast_in_dim.40), channel_id=1, replica_groups=mesh['sp'=64,'tp'=8] {'tp'}, dimensions={0} | all-to-all | bytes 3391488 | tf_op jit(solution)/shard_map/all_to_all | solution.py:42
  148.1 1.0 copy.21
  149.1 0.1 pad.11
  149.2 0.5 copy.32
  149.7 1.9 add_convert_fusion
  151.6 1.3 broadcast_in_dim.42
  152.9 4.4 %all-to-all-start.3 = ((bf16[8,414,256]{2,1,0:T(8,128)(2,1)}), bf16[8,414,256]{2,1,0:T(8,128)(2,1)S(1)}, u32[]{:S(2)}, u32[]{:S(2)}) async-start(bf16[8,414,256]{2,1,0:T(8,128)(2,1)} %broadcast_in_dim.42), calls=%async_computation.3 | async-start | bytes 3407872 | tf_op jit(solution)/shard_map/all_to_all | solution.py:42
  157.3 22.0 %all-to-all-done.3 = bf16[8,414,256]{2,1,0:T(8,128)(2,1)S(1)} async-done(((bf16[8,414,256]{2,1,0:T(8,128)(2,1)}), bf16[8,414,256]{2,1,0:T(8,128)(2,1)S(1)}, u32[]{:S(2)}, u32[]{:S(2)}) %all-to-all-start.3) | async-done | bytes 1695776 | tf_op jit(solution)/shard_map/all_to_all | solution.py:42
  179.3 0.4 fusion.3
  179.7 0.5 fusion.7
  180.2 1.0 copy.22
  181.1 0.1 pad.12
  181.3 0.5 copy.33
  181.8 1.9 fusion.14
  183.7 1.9 fusion.17
  185.5 1.7 fusion.27
  187.3 8.0 %all_to_all.33 = f32[8,1,768]{2,1,0:T(1,128)S(1)} all-to-all(f32[8,1,768]{2,1,0:T(1,128)S(1)} %broadcast_in_dim.72), channel_id=1, replica_groups=mesh['sp'=64,'tp'=8] {'tp'}, dimensions={0} | all-to-all | bytes 49152 | tf_op jit(solution)/shard_map/all_to_all | solution.py:42
  195.3 0.2 multiply_convert_fusion.1
  195.6 0.2 copy.24
  195.7 0.1 broadcast_in_dim.73
  195.9 23.7 %all_to_all.34 = bf16[8,384,256]{1,2,0:T(8,128)(2,1)S(1)} all-to-all(bf16[8,384,256]{1,2,0:T(8,128)(2,1)S(1)} %broadcast_in_dim.73), channel_id=1, replica_groups=mesh['sp'=64,'tp'=8] {'tp'}, dimensions={0} | all-to-all | bytes 3145728 | tf_op jit(solution)/shard_map/all_to_all | solution.py:42
  219.6 2.5 %fusion.18 = bf16[384,256]{1,0:T(8,128)(2,1)} fusion(bf16[384,2048]{0,1:T(8,128)(2,1)S(1)} %bitcast.120, bf16[6,2048,256]{2,1,0:T(8,128)(2,1)} %all-gather.2.cloned.1.call-done, bf16[414,256]{1,0:T(8,128)(2,1)S(1)} %add_convert_fusion), kind=kOutput, calls=%fused_computation.27 | convolution fusion | flops 402948096 | bytes 3014656 | tf_op jit(solution)/shard_map/dot_general | solution.py:119
  (19 shorter events, 0.3 us)
Async XLA Ops:
  6.5 98.7 %all-gather.2.cloned.1.call-start = ((), (), s32[]{:S(2)}) async-start(), calls=%async_computation.6 | async-start | bytes 6389760 | tf_op jit(solution)/shard_map/all_gather | solution.py:18
  8.8 5.9 %collective-permute-start.1 = (bf16[30,256]{1,0:T(8,128)(2,1)S(1)}, bf16[30,256]{1,0:T(8,128)(2,1)S(1)}, u32[]{:S(2)}, u32[]{:S(2)}) collective-permute-start(bf16[30,256]{1,0:T(8,128)(2,1)S(1)} %get-tuple-element.14), channel_id=1, source_target_pairs={{8,0},{16,8},{24,16},{32,24},{40,32},{48,40},{56,48},{64,56},{72,6... | collective-permute-start | bytes 46088 | tf_op jit(solution)/shard_map/ppermute | solution.py:29
  10.0 5.5 %collective-permute-start = (bf16[30,256]{1,0:T(8,128)(2,1)S(1)}, bf16[30,256]{1,0:T(8,128)(2,1)S(1)}, u32[]{:S(2)}, u32[]{:S(2)}) collective-permute-start(bf16[30,256]{1,0:T(8,128)(2,1)S(1)} %get-tuple-element.13), channel_id=1, source_target_pairs={{0,8},{8,16},{16,24},{24,32},{32,40},{40,48},{48,56},{56,64},{64,7... | collective-permute-start | bytes 46088 | tf_op jit(solution)/shard_map/ppermute | solution.py:26
  17.9 11.0 %copy-start.1 = (f32[2,2048]{1,0:T(2,128)S(1)}, f32[2,2048]{1,0:T(2,128)}, u32[]{:S(2)}) copy-start(f32[2,2048]{1,0:T(2,128)} %param.10) | copy-start | bytes 49156
  17.9 11.0 %copy-start.2 = (f32[2,256]{1,0:T(2,128)S(1)}, f32[2,256]{1,0:T(2,128)}, u32[]{:S(2)}) copy-start(f32[2,256]{1,0:T(2,128)} %param.14) | copy-start | bytes 6148
  17.9 11.1 %copy-start.3 = (f32[2,256]{1,0:T(2,128)S(1)}, f32[2,256]{1,0:T(2,128)}, u32[]{:S(2)}) copy-start(f32[2,256]{1,0:T(2,128)} %param.16) | copy-start | bytes 6148
  17.9 11.1 %copy-start = (f32[2,31,256]{2,0,1:T(2,128)S(1)}, f32[2,31,256]{2,0,1:T(2,128)}, u32[]{:S(2)}) copy-start(f32[2,31,256]{2,0,1:T(2,128)} %param.13) | copy-start | bytes 190468
  17.9 34.4 %all-to-all-start = ((bf16[8,444,256]{2,1,0:T(8,128)(2,1)}), bf16[8,444,256]{2,1,0:T(8,128)(2,1)S(1)}, u32[]{:S(2)}, u32[]{:S(2)}) async-start(bf16[8,444,256]{2,1,0:T(8,128)(2,1)} %broadcast_in_dim.37), calls=%async_computation | async-start | bytes 3670016 | tf_op jit(solution)/shard_map/all_to_all | solution.py:42
  109.0 8.7 %copy-start.4 = (f32[2,256]{1,0:T(2,128)S(1)}, f32[2,256]{1,0:T(2,128)}, u32[]{:S(2)}) copy-start(f32[2,256]{1,0:T(2,128)} %param.15) | copy-start | bytes 6148
  111.5 10.8 %all-to-all-start.1 = ((f32[8,1,828]{2,1,0:T(1,128)}), f32[8,1,828]{2,1,0:T(1,128)S(1)}, u32[]{:S(2)}, u32[]{:S(2)}) async-start(f32[8,1,828]{2,1,0:T(1,128)} %broadcast_in_dim.39), calls=%async_computation.1 | async-start | bytes 57344 | tf_op jit(solution)/shard_map/all_to_all | solution.py:42
  152.9 26.4 %all-to-all-start.3 = ((bf16[8,414,256]{2,1,0:T(8,128)(2,1)}), bf16[8,414,256]{2,1,0:T(8,128)(2,1)S(1)}, u32[]{:S(2)}, u32[]{:S(2)}) async-start(bf16[8,414,256]{2,1,0:T(8,128)(2,1)} %broadcast_in_dim.42), calls=%async_computation.3 | async-start | bytes 3407872 | tf_op jit(solution)/shard_map/all_to_all | solution.py:42
Sparse Core Ops, SparseCore 0:
  10.3 94.7 all-gather.1
where the time goes:
time: 230 us; the launch traced here: 229 us
  waiting for transfers between devices  101 us (44%)
  blocking collectives  57 us (25%)
  starting transfers between devices  27.4 us (12%)
  between operations  13.7 us (6%)
  matrix products  11.9 us (5%)
  local copies, waits for them, and re-layouts  9.55 us (4%)
  other arithmetic  8.57 us (4%)
    all_to_all x3, blocking collectives, from_everyone(): lax.all_to_all(jnp.broadcast_to(x[None], (length, *x.shape)), axis, 0, 0,...  57 us
    all_gather x1, waiting for transfers between devices, in_one_piece(): lax.all_gather(both, axis, axis=dim, tiled=True)  50.2 us
    all_to_all x3, waiting for transfers between devices, from_everyone(): lax.all_to_all(jnp.broadcast_to(x[None], (length, *x.shape)), axis, 0, 0,...  49.9 us
    all_to_all x3, starting transfers between devices, from_everyone(): lax.all_to_all(jnp.broadcast_to(x[None], (length, *x.shape)), axis, 0, 0,...  21.4 us
    ppermute x1, starting transfers between devices, with_halo(): lax.ppermute(lax.slice_in_dim(block, block.shape[dim] - width, None, axis...  4.65 us
  transfers between devices with their start and end apart: 6, of which 5 were waited for; matrix products, arithmetic and copies ran while one was open for 3% of the time, Pallas kernels for 0%

commit v1 on v0

v1 whole, which is shorter than its diff:
```python
import functools

import jax
import jax.numpy as jnp
from jax import lax
from jax.experimental import pallas as pl
from jax.experimental.pallas import tpu as pltpu
from jax.sharding import PartitionSpec as P

EPSILON = 1e-06
MESH = pl.DeviceIdType.MESH
C = 256
HALO = 32
BLK = 32
SUB = (2, 1, 2, 1)
ITEMS = [(st, h) for st in range(4) for h in range(SUB[st])]


def remote(src, dst, ssem, rsem, dev):
    return pltpu.make_async_remote_copy(
        src_ref=src, dst_ref=dst, send_sem=ssem, recv_sem=rsem, device_id=dev, device_id_type=MESH
    )


def kernel(
    nz, ny, nx, tokens, width,
    stream, a_w, g_w, o_w, norm_gain, conv_w, conv_b, ln_gain, ln_shift,
    out,
    wag, wo, xb0, xb1, mb0, mb1, u, gs, acc, ss, st, so, sb, q, qt, lno, lnb,
    p1_s, p1_r, rg_s, rg_r, xg_s, xg_r, dd_s, dd_r, do_s, do_r, hl_s, hl_r, st_s, st_r, ln_s, ln_r, loc,
):
    tp = 2 * nx
    sp_n = nz * ny
    d_model = C * tp
    kb = d_model // sp_n
    sp = lax.axis_index("sp")
    me = lax.axis_index("tp")
    z, y = sp // ny, lax.rem(sp, ny)
    x, core = me // 2, lax.rem(me, 2)
    sib = me + 1 - 2 * core
    r0, r1, r2 = tokens + 2 * HALO, tokens + HALO, tokens

    def spid(zz, yy):
        return lax.rem(zz, nz) * ny + lax.rem(yy, ny)

    def rel(j):
        qq, c = j // 2, j % 2
        dx = jnp.where(qq == 0, 0, jnp.where(qq == 1, nx - 1, jnp.where(qq == 2, 1, 2)))
        return lax.rem(x + dx, nx) * 2 + lax.rem(core + c, 2)

    peers = [lax.rem(me + j, tp) for j in range(1, tp)]
    nxt, prv = lax.rem(sp + 1, sp_n), lax.rem(sp + sp_n - 1, sp_n)

    barrier = pltpu.get_barrier_semaphore()

    def greet(dev):
        pl.semaphore_signal(barrier, inc=1, device_id=dev, device_id_type=MESH)

    for j in range(1, ny):
        greet((spid(z, y + j), me))
    for j in range(1, nz):
        greet((spid(z + j, y), me))
    greet((nxt, me))
    greet((prv, me))
    for p in peers:
        greet((sp, p))

    local = [pltpu.make_async_copy(stream, xb0.at[me, pl.ds(HALO, tokens)], loc.at[0])]
    n = 1
    for l in range(2):
        for h in range(2):
            src = pl.ds(128 * h, 128)
            local.append(pltpu.make_async_copy(
                a_w.at[l, :, src], wag.at[l, z, y, :, pl.ds(256 * h, 128)], loc.at[n]))
            local.append(pltpu.make_async_copy(
                g_w.at[l, :, src], wag.at[l, z, y, :, pl.ds(256 * h + 128, 128)], loc.at[n + 1]))
            n += 2
        local.append(pltpu.make_async_copy(o_w.at[l], wo.at[l, z, y], loc.at[n]))
        n += 1
    for c in local:
        c.start()
    lno[...] = jnp.zeros_like(lno)
    lno[0:2, :] = ln_gain[...]
    lno[2:4, :] = ln_shift[...]
    lnb[me] = lno[...]
    for c in local:
        c.wait()
    pl.semaphore_wait(barrier, ny + nz + tp - 1)

    def weight(stage, path):
        buf, cols = (wag, 256) if stage % 2 == 0 else (wo, 128)
        return buf.at[stage // 2], pl.ds(cols * path, cols)

    def first_send(stage):
        for path in range(2):
            ref, cols = weight(stage, path)
            mine = ref.at[z, y, :, cols]
            for j in range(1, ny if path == 0 else nz):
                to = spid(z, y + j) if path == 0 else spid(z + j, y)
                remote(mine, mine, p1_s.at[path, stage], p1_r.at[path, stage], (to, me)).start()

    def first_all(stage, path):
        ref, cols = weight(stage, path)
        if path == 0:
            return ref.at[0, pl.ds(0, ny - 1), :, cols]
        return ref.at[pl.ds(0, nz - 1), 0, :, cols]

    def first_wait(stage):
        for path in range(2):
            whole = first_all(stage, path)
            remote(whole, whole, p1_s.at[path, stage], p1_r.at[path, stage], (sp, sib)).wait_recv()

    def ring_block(item, path, origin):
        stage, h = ITEMS[item]
        ref, cols = weight(stage, path)
        if path == 0:
            m = ny // SUB[stage]
            return ref.at[origin, pl.ds(h * m, m), :, cols]
        m = nz // SUB[stage]
        return ref.at[pl.ds(h * m, m), origin, :, cols]

    def ring_hops(item, path, way):
        size = nz if path == 0 else ny
        return size // 2 if (item + way) % 2 == 0 else size - 1 - size // 2

    def ring_copy(item, path, way, hop, origin):
        step = 1 if way == 0 else -1
        if path == 0:
            to = spid(z + nz + step, y)
        else:
            to = spid(z, y + ny + step)
        block = ring_block(item, path, origin)
        return remote(block, block, rg_s.at[path, way, item], rg_r.at[path, way, item, hop], (to, me))

    def ring(stage, hop):
        for item, (of, _) in enumerate(ITEMS):
            if of != stage:
                continue
            for path in range(2):
                size, at = (nz, z) if path == 0 else (ny, y)
                for way in range(2):
                    hops = ring_hops(item, path, way)
                    step = 1 if way == 0 else -1
                    origin = lax.rem(at + 2 * size - step * hop, size)
                    if 0 < hop <= hops:
                        ring_copy(item, path, way, hop - 1, origin).wait_recv()
                    if hop < hops:
                        ring_copy(item, path, way, hop, origin).start()

    def ring_drain():
        for item, (stage, _) in enumerate(ITEMS):
            for path in range(2):
                ref, cols = weight(stage, path)
                for way in range(2):
                    hops = ring_hops(item, path, way)
                    if hops == 0:
                        continue
                    if path == 0:
                        whole = ref.at[pl.ds(0, hops), pl.ds(0, ny // SUB[stage]), :, cols]
                    else:
                        whole = ref.at[pl.ds(0, nz // SUB[stage]), pl.ds(0, hops), :, cols]
                    remote(whole, whole, rg_s.at[path, way, item], rg_s.at[path, way, item], (sp, sib)).wait_send()
        for stage in range(4):
            for path in range(2):
                whole = first_all(stage, path)
                remote(whole, whole, p1_s.at[path, stage], p1_r.at[path, stage], (sp, sib)).wait_send()

    def x_hops(half, way):
        return nx // 2 if (half + way) % 2 == 0 else nx - 1 - nx // 2

    def x_order(way):
        return (0, 1) if way == 0 else (1, 0)

    def x_piece(buf, rows, half, owner):
        cut = (rows // 2 + BLK - 1) // BLK * BLK
        return buf.at[owner, pl.ds(0, cut) if half == 0 else pl.ds(cut, rows - cut)]

    def x_owner(way, hop):
        step = 1 if way == 0 else -1
        return lax.rem(x + 2 * nx - step * hop, nx) * 2 + core

    def x_copy(g, buf, rows, half, way, hop):
        step = 1 if way == 0 else -1
        to = lax.rem(x + nx + step, nx) * 2 + core
        piece = x_piece(buf, rows, half, x_owner(way, hop))
        return remote(piece, piece, xg_s.at[g, way, half, hop], xg_r.at[g, way, half, hop], (sp, to))

    def d_copy(g, buf, rows, half, way, hop):
        piece = x_piece(buf, rows, half, x_owner(way, hop))
        return remote(piece, piece, dd_s.at[g, way, half, hop - 1], dd_r.at[g, way, half, hop - 1], (sp, sib))

    def own_copy(g, buf, rows):
        piece = buf.at[me, pl.ds(0, rows)]
        return remote(piece, piece, do_s.at[g], do_r.at[g], (sp, sib))

    def x_pieces(hop):
        return [(half, way) for k in range(2) for way in range(2)
                for half in (x_order(way)[k],) if hop <= x_hops(half, way)]

    def gather_start(g, buf, rows):
        for half, way in x_pieces(1):
            x_copy(g, buf, rows, half, way, 0).start()
        own_copy(g, buf, rows).start()

    def gather_hop(g, buf, rows, hop):
        for half, way in x_pieces(hop):
            x_copy(g, buf, rows, half, way, hop - 1).wait_recv()
            if hop < x_hops(half, way):
                x_copy(g, buf, rows, half, way, hop).start()
            d_copy(g, buf, rows, half, way, hop).start()

    def gather_pair(g, buf, rows, hop):
        for half, way in x_pieces(hop):
            d_copy(g, buf, rows, half, way, hop).wait_recv()

    def gather_drain(g, buf, rows):
        own_copy(g, buf, rows).wait_send()
        for hop in range(1, nx // 2 + 1):
            for half, way in x_pieces(hop):
                x_copy(g, buf, rows, half, way, hop - 1).wait_send()
                d_copy(g, buf, rows, half, way, hop).wait_send()

    def blocks(rows, body):
        def run(b, carry):
            body(pl.multiple_of(b * BLK, BLK))
            return carry
        lax.fori_loop(0, rows // BLK, run, 0)

    def wide(ref, l, p):
        return ref[l, p].reshape(C, ref.shape[-1])

    def matmul(l, ref, rows, lo, hi):
        cols = ref.shape[-1]

        def run(j, carry):
            part = jnp.dot(u[j, 0:rows, :], wide(ref, l, rel(j)), preferred_element_type=jnp.float32)
            acc[0:rows, 0:cols] = acc[0:rows, 0:cols] + part
            return carry
        lax.fori_loop(lo, hi, run, 0)

    def clear(rows):
        def body(i):
            acc[pl.ds(i, BLK), :] = jnp.zeros((BLK, 2 * C), jnp.float32)
        blocks(rows, body)

    def prepare(l, buf, rows, lo, hi):
        def run(j, carry):
            p = rel(j)
            gain = norm_gain[l, p]

            def body(i):
                v = buf[p, pl.ds(i, BLK), :].astype(jnp.float32)
                sq = v * v
                part = sq[:, 0:128] + sq[:, 128:256]
                ss[pl.ds(i, BLK), :] = ss[pl.ds(i, BLK), :] + part
                u[j, pl.ds(i, BLK), :] = (v * gain).astype(jnp.bfloat16)
            blocks(rows, body)
            return carry
        lax.fori_loop(lo, hi, run, 0)

    def clear_squares(rows):
        def body(i):
            ss[pl.ds(i, BLK), :] = jnp.zeros((BLK, 128), jnp.float32)
        blocks(rows, body)

    def gate(rows, margin):
        def body(i):
            total = jnp.sum(ss[pl.ds(i, BLK), :], axis=1, keepdims=True)
            factor = lax.rsqrt(total * (1.0 / d_model) + EPSILON)
            at = sp * tokens - margin + i + lax.broadcasted_iota(jnp.int32, (BLK, 128), 0)
            inside = (at >= 0) & (at < tokens * sp_n)
            for h in range(2):
                lin = acc[pl.ds(i, BLK), 256 * h:256 * h + 128] * factor
                gat = acc[pl.ds(i, BLK), 256 * h + 128:256 * h + 256] * factor
                val = jnp.where(inside, lin * jax.nn.sigmoid(gat), 0.0)
                gs[h, pl.ds(i, BLK), :] = val.astype(jnp.bfloat16).astype(jnp.float32)
        blocks(rows, body)

    def convolve(l, buf, rows):
        lane = lax.broadcasted_iota(jnp.int32, (BLK, 128), 1)

        def body(i):
            sums = []
            for h in range(2):
                cols = slice(128 * h, 128 * h + 128)
                total = jnp.broadcast_to(conv_b[l, :, cols], (BLK, 128))
                for k in range(width):
                    total = total + gs[h, pl.ds(i + (1 + k), BLK), :] * conv_w[l, k:k + 1, cols]
                sums.append(total)
            mean = jnp.sum(sums[0] + sums[1], axis=1, keepdims=True) * (1.0 / C)
            low, high = sums[0] - mean, sums[1] - mean
            spread = jnp.sum(low * low + high * high, axis=1, keepdims=True)
            buf[me, pl.ds(i, BLK), 0:128] = low.astype(jnp.bfloat16)
            buf[me, pl.ds(i, BLK), 128:256] = high.astype(jnp.bfloat16)
            st[pl.ds(i, BLK), :] = jnp.where(lane == 0, mean, jnp.where(lane == 1, spread, 0.0))
        blocks(rows, body)

    def stats_send(l):
        so[l] = st[...].T[0:8, :]
        sb[l, me] = so[l]
        for p in peers:
            remote(so.at[l], sb.at[l, me], st_s.at[l], st_r.at[l], (sp, p)).start()

    def stats_all(l):
        whole = sb.at[l, pl.ds(0, tp - 1)]
        return remote(whole, whole, st_s.at[l], st_r.at[l], (sp, sib))

    def stats_take(l):
        stats_all(l).wait_recv()
        means = [sb[l, rel(j), 0:1, :] for j in range(tp)]
        spreads = [sb[l, rel(j), 1:2, :] for j in range(tp)]
        average = sum(means) * (1.0 / tp)
        apart = [m - average for m in means]
        variance = sum(spreads) * (1.0 / d_model) + sum(v * v for v in apart) * (1.0 / tp)
        q[0:tp, :] = jnp.concatenate(apart, axis=0)
        q[tp:tp + 8, :] = jnp.broadcast_to(lax.rsqrt(variance + EPSILON), (8, q.shape[1]))
        qt[...] = q[...].T

    def mix(l, buf, rows, js):
        for j in js:
            p = rel(j)
            gain = lnb[p, l:l + 1, :]
            shift = lnb[p, 2 + l:3 + l, :]

            def body(i):
                v = buf[p, pl.ds(i, BLK), :].astype(jnp.float32)
                v = (v + qt[pl.ds(i, BLK), j:j + 1]) * qt[pl.ds(i, BLK), tp:tp + 1] * gain + shift
                u[j, pl.ds(i, BLK), :] = (v * jax.nn.sigmoid(v)).astype(jnp.bfloat16)
            blocks(rows, body)

    def finish(src, rows, skip, dst):
        def body(i):
            old = src[me, pl.ds(pl.multiple_of(i + skip, 16), BLK), :].astype(jnp.float32)
            dst[pl.ds(i, BLK), :] = (old + acc[pl.ds(i, BLK), 0:C]).astype(jnp.bfloat16)
        blocks(rows, body)

    near = min(6, tp)

    halo = [
        remote(xb0.at[me, pl.ds(HALO, HALO)], xb0.at[me, pl.ds(HALO + tokens, HALO)],
               hl_s.at[0], hl_r.at[0], (prv, me)),
        remote(xb0.at[me, pl.ds(tokens, HALO)], xb0.at[me, pl.ds(0, HALO)],
               hl_s.at[1], hl_r.at[1], (nxt, me)),
    ]
    for c in halo:
        c.start()
    first_send(0)
    for p in peers:
        remote(lno, lnb.at[me], ln_s.at[0], ln_r.at[0], (sp, p)).start()
    ln_all = remote(lnb.at[pl.ds(0, tp - 1)], lnb.at[pl.ds(0, tp - 1)], ln_s.at[0], ln_r.at[0], (sp, sib))
    clear(r0)
    clear_squares(r0)
    for c in halo:
        c.wait_recv()
    gather_start(0, xb0, r0)
    first_send(1)
    prepare(0, xb0, r0, 0, 1)
    first_wait(0)
    ring(0, 0)
    first_send(2)
    gather_hop(0, xb0, r0, 1)
    first_wait(1)
    ring(1, 0)
    ring(0, 1)
    first_send(3)
    own_copy(0, xb0, r0).wait_recv()
    gather_pair(0, xb0, r0, 1)
    prepare(0, xb0, r0, 1, near)
    ring(0, 2)
    for hop in range(2, nx // 2 + 1):
        gather_hop(0, xb0, r0, hop)
        gather_pair(0, xb0, r0, hop)
    prepare(0, xb0, r0, near, tp)
    ring(0, 3)
    ring(1, 1)
    first_wait(2)
    ring(2, 0)
    ring(0, 4)
    matmul(0, wag, r0, 0, tp)
    ring(1, 2)
    gate(r0, HALO)
    ring(2, 1)
    convolve(0, mb0, r1)
    stats_send(0)
    gather_start(1, mb0, r1)
    ring(1, 3)
    ring(1, 4)
    first_wait(3)
    ring(3, 0)
    ring(2, 2)
    clear(r1)
    ln_all.wait_recv()
    stats_take(0)
    mix(0, mb0, r1, [0])
    gather_hop(1, mb0, r1, 1)
    ring(2, 3)
    own_copy(1, mb0, r1).wait_recv()
    gather_pair(1, mb0, r1, 1)
    mix(0, mb0, r1, range(1, near))
    matmul(0, wo, r1, 0, near)
    for hop in range(2, nx // 2 + 1):
        gather_hop(1, mb0, r1, hop)
        gather_pair(1, mb0, r1, hop)
    mix(0, mb0, r1, range(near, tp))
    matmul(0, wo, r1, near, tp)
    finish(xb0, r1, 16, xb1.at[me])
    gather_start(2, xb1, r1)
    ring(2, 4)
    ring(3, 1)
    clear(r1)
    clear_squares(r1)
    prepare(1, xb1, r1, 0, 1)
    matmul(1, wag, r1, 0, 1)
    ring(3, 2)
    gather_hop(2, xb1, r1, 1)
    ring(3, 3)
    own_copy(2, xb1, r1).wait_recv()
    gather_pair(2, xb1, r1, 1)
    prepare(1, xb1, r1, 1, near)
    matmul(1, wag, r1, 1, near)
    for hop in range(2, nx // 2 + 1):
        gather_hop(2, xb1, r1, hop)
        gather_pair(2, xb1, r1, hop)
    prepare(1, xb1, r1, near, tp)
    matmul(1, wag, r1, near, tp)
    gate(r1, HALO // 2)
    convolve(1, mb1, r2)
    stats_send(1)
    gather_start(3, mb1, r2)
    ring(3, 4)
    clear(r2)
    stats_take(1)
    mix(1, mb1, r2, [0])
    gather_hop(3, mb1, r2, 1)
    own_copy(3, mb1, r2).wait_recv()
    gather_pair(3, mb1, r2, 1)
    mix(1, mb1, r2, range(1, near))
    matmul(1, wo, r2, 0, near)
    for hop in range(2, nx // 2 + 1):
        gather_hop(3, mb1, r2, hop)
        gather_pair(3, mb1, r2, hop)
    mix(1, mb1, r2, range(near, tp))
    matmul(1, wo, r2, near, tp)
    finish(xb1, r2, 16, out)

    ring_drain()
    gather_drain(0, xb0, r0)
    gather_drain(1, mb0, r1)
    gather_drain(2, xb1, r1)
    gather_drain(3, mb1, r2)
    for c in halo:
        c.wait_send()
    stats_all(0).wait_send()
    stats_all(1).wait_send()
    ln_all.wait_send()


def build(mesh, nz, ny, nx):
    tp = 2 * nx
    spec = (
        P("sp", "tp"), P(), P(None, "sp", "tp"), P(None, "sp", "tp"), P(None, None, "tp"),
        P(None, "tp"), P(None, "tp"), P(None, "tp"), P(None, "sp", "tp"),
    )

    def local(stream, norm_gain, a_w, g_w, conv_w, conv_b, ln_gain, ln_shift, o_w):
        tokens = stream.shape[0]
        width = conv_w.shape[1]
        kb = a_w.shape[1]
        r0, r1, r2 = tokens + 2 * HALO, tokens + HALO, tokens
        lanes = (r1 + 127) // 128 * 128
        dma, f32, b16 = pltpu.SemaphoreType.DMA, jnp.float32, jnp.bfloat16
        hops = max(nz, ny) // 2
        anywhere = pl.BlockSpec(memory_space=pl.ANY)
        inside = pl.BlockSpec(memory_space=pltpu.VMEM)
        return pl.pallas_call(
            functools.partial(kernel, nz, ny, nx, tokens, width),
            out_shape=jax.ShapeDtypeStruct((tokens, C), b16),
            in_specs=[anywhere] * 4 + [inside] * 5,
            out_specs=inside,
            scratch_shapes=[
                pltpu.VMEM((2, nz, ny, kb, 2 * C), b16),
                pltpu.VMEM((2, nz, ny, kb, C), b16),
                pltpu.VMEM((tp, r0, C), b16),
                pltpu.VMEM((tp, r1, C), b16),
                pltpu.VMEM((tp, r1, C), b16),
                pltpu.VMEM((tp, r2, C), b16),
                pltpu.VMEM((tp, r0, C), b16),
                pltpu.VMEM((2, r0 + BLK, 128), f32),
                pltpu.VMEM((r0, 2 * C), f32),
                pltpu.VMEM((r0, 128), f32),
                pltpu.VMEM((lanes, 128), f32),
                pltpu.VMEM((2, 8, lanes), f32),
                pltpu.VMEM((2, tp, 8, lanes), f32),
                pltpu.VMEM((128, lanes), f32),
                pltpu.VMEM((lanes, 128), f32),
                pltpu.VMEM((8, C), f32),
                pltpu.VMEM((tp, 8, C), f32),
                dma((2, 4)), dma((2, 4)),
                dma((2, 2, len(ITEMS))), dma((2, 2, len(ITEMS), hops)),
                dma((4, 2, 2, 2)), dma((4, 2, 2, 2)),
                dma((4, 2, 2, 2)), dma((4, 2, 2, 2)),
                dma((4,)), dma((4,)),
                dma((2,)), dma((2,)),
                dma((2,)), dma((2,)),
                dma((1,)), dma((1,)),
                dma((16,)),
            ],
            compiler_params=pltpu.CompilerParams(
                collective_id=0, has_side_effects=True, vmem_limit_bytes=56 * 1024 * 1024
            ),
        )(
            stream, a_w, g_w, o_w, norm_gain.reshape(2, tp, 1, C), conv_w,
            conv_b.reshape(2, 1, C), ln_gain, ln_shift,
        )

    return jax.shard_map(local, mesh=mesh, in_specs=spec, out_specs=P("sp", "tp"), check_vma=False)


def solution(mesh):
    return build(mesh, 8, 8, 4)
```

time: 230 us -> 119 us (0.52)
  Pallas kernels: 0 us -> 113 us
  waiting for transfers between devices: 101 us -> 0 us
  blocking collectives: 57 us -> 0 us
  starting transfers between devices: 27.4 us -> 0 us
  between operations: 13.7 us -> 0.01 us
  matrix products: 11.9 us -> 0 us
  other arithmetic: 8.57 us -> 0 us
  local copies, waits for them, and re-layouts: 9.55 us -> 5.67 us
    pallas_call x0 -> x1, Pallas kernels: none -> 113 us  [local(): pl.pallas_call(functools.partial(kernel, nz, ny, nx, tokens, width), out_...]
    all_to_all x3 -> x0, blocking collectives: 57 us -> none  [from_everyone(): lax.all_to_all(jnp.broadcast_to(x[None], (length, *x.shape)), axis, 0, 0,...]
    all_gather x1 -> x0, waiting for transfers between devices: 50.2 us -> none  [in_one_piece(): lax.all_gather(both, axis, axis=dim, tiled=True)]
    all_to_all x3 -> x0, waiting for transfers between devices: 49.9 us -> none  [from_everyone(): lax.all_to_all(jnp.broadcast_to(x[None], (length, *x.shape)), axis, 0, 0,...]
    all_to_all x3 -> x0, starting transfers between devices: 21.4 us -> none  [from_everyone(): lax.all_to_all(jnp.broadcast_to(x[None], (length, *x.shape)), axis, 0, 0,...]
    dot_general x6 -> x0, matrix products: 11.9 us -> none  [the longest x2 4.38 us: local(): jnp.dot(mixed_rows, gathered[2][layer_index], preferred_element_type=jnp....]
    ppermute x2 -> x0, starting transfers between devices: 5.93 us -> none  [the longest x1 4.65 us: with_halo(): lax.ppermute(lax.slice_in_dim(block, block.shape[dim] - width, None, axis...]
    reduce_sum x6 -> x0, other arithmetic: 4.5 us -> none  [the longest x2 3.58 us: local(): jnp.sum(conv_out, axis=1, keepdims=True)]
  transfers between devices with their start and end apart: 6 -> 0, of which waited for: 5 -> 0; matrix products, arithmetic and copies ran while one was open for 3% -> 0% of each run, Pallas kernels for 0% -> 0%
where the time goes in v1:
time: 119 us
  Pallas kernels  113 us (95%)
  local copies, waits for them, and re-layouts  5.67 us (5%)
    pallas_call x1, Pallas kernels, local(): pl.pallas_call(functools.partial(kernel, nz, ny, nx, tokens, width), out_...  113 us
    unnamed x2, local copies, waits for them, and re-layouts  3.08 us

profile of v1, /device:TPU:1, one launch (start us, length us, event | category | flops | bytes accessed | tf_op | source)
XLA Modules:
  0.0 119.1 jit_solution(4692688432026766675)
XLA Ops:
  0.0 1.2 %reshape.7.conv_b = f32[2,1,256]{2,1,0:T(1,128)} reshape(f32[2,256]{1,0:T(2,128)} %param.14) | data formatting | bytes 4096 | tf_op jit(solution)/shard_map/reshape | solution.py:513
  1.2 1.3 %reshape.6.norm_gain = f32[2,8,1,256]{3,2,1,0:T(1,128)} reshape(f32[2,2048]{1,0:T(2,128)} %param.10) | data formatting | bytes 32768 | tf_op jit(solution)/shard_map/reshape | solution.py:512
  2.6 1.5 %copy.10.conv_w = f32[2,31,256]{2,1,0:T(8,128)} copy(f32[2,31,256]{2,0,1:T(2,128)} %param.13) | data formatting | bytes 126976 | tf_op args[4]
  4.1 113.4 %shard_map.91 = bf16[384,256]{1,0:T(8,128)(2,1)} custom-call(bf16[384,256]{1,0:T(8,128)(2,1)} %stream.1, bf16[2,32,256]{2,1,0:T(8,128)(2,1)} %a_w.1, bf16[2,32,256]{2,1,0:T(8,128)(2,1)} %g_w.1, bf16[2,32,256]{2,1,0:T(8,128)(2,1)} %o_w.1, f32[2,8,1,256]{3,2,1,0:T(1,128)} %reshape.6.norm_gain, f32[2,31,256]{2,1,0:T(8,128)} %copy.10.conv_w, ...), custom_call_target="tpu_custom_call" | custom-call | tf_op jit(solution)/shard_map/pallas_call | solution.py:475
  117.5 1.6 %copy.12 = bf16[384,256]{1,0:T(8,128)(2,1)} copy(bf16[384,256]{1,0:T(8,128)(2,1)} %shard_map.91) | data formatting | bytes 393216

commit v2 on v1

--- a/solution.py
+++ b/solution.py
@@ -12,7 +12,7 @@
 C = 256
 HALO = 32
 BLK = 32
-SUB = (2, 1, 2, 1)
+SUB = (4, 2, 4, 2)
 ITEMS = [(st, h) for st in range(4) for h in range(SUB[st])]
 
 
@@ -42,11 +42,6 @@
 
     def spid(zz, yy):
         return lax.rem(zz, nz) * ny + lax.rem(yy, ny)
-
-    def rel(j):
-        qq, c = j // 2, j % 2
-        dx = jnp.where(qq == 0, 0, jnp.where(qq == 1, nx - 1, jnp.where(qq == 2, 1, 2)))
-        return lax.rem(x + dx, nx) * 2 + lax.rem(core + c, 2)
 
     peers = [lax.rem(me + j, tp) for j in range(1, tp)]
     nxt, prv = lax.rem(sp + 1, sp_n), lax.rem(sp + sp_n - 1, sp_n)
@@ -221,59 +216,75 @@
                 d_copy(g, buf, rows, half, way, hop).wait_send()
 
     def blocks(rows, body):
-        def run(b, carry):
-            body(pl.multiple_of(b * BLK, BLK))
+        for i in range(0, rows, BLK):
+            body(i)
+
+    def pair_chip(k):
+        return lax.rem(x + (0, nx - 1, 1, 2)[k], nx)
+
+    def each(k, body):
+        def run(c, carry):
+            body(pair_chip(k) * 2 + c)
             return carry
-        lax.fori_loop(0, rows // BLK, run, 0)
-
-    def wide(ref, l, p):
-        return ref[l, p].reshape(C, ref.shape[-1])
-
-    def matmul(l, ref, rows, lo, hi):
+        lax.fori_loop(0, 2, run, 0)
+
+    def lanes(p):
+        return pl.ds(pl.multiple_of(p * C, C), C)
+
+    def matmul(l, ref, rows, ks):
         cols = ref.shape[-1]
-
-        def run(j, carry):
-            part = jnp.dot(u[j, 0:rows, :], wide(ref, l, rel(j)), preferred_element_type=jnp.float32)
-            acc[0:rows, 0:cols] = acc[0:rows, 0:cols] + part
-            return carry
-        lax.fori_loop(lo, hi, run, 0)
-
-    def clear(rows):
+        for k in ks:
+            chip = pair_chip(k)
+            left = u[0:rows, pl.ds(pl.multiple_of(chip * 2 * C, 2 * C), 2 * C)]
+            right = ref[l, pl.ds(chip * 2, 2)].reshape(2 * C, cols)
+            part = jnp.dot(left, right, preferred_element_type=jnp.float32)
+            if k == 0:
+                acc[0:rows, 0:cols] = part
+            else:
+                acc[0:rows, 0:cols] = acc[0:rows, 0:cols] + part
+
+    def matmul_whole(l, ref, rows):
+        cols = ref.shape[-1]
+        for h in range(cols // C):
+            right = ref[l, :, :, :, C * h:C * h + C].reshape(d_model, C)
+            acc[0:rows, C * h:C * h + C] = jnp.dot(
+                u[0:rows, :], right, preferred_element_type=jnp.float32)
+
+    def prepare(l, buf, rows, k):
+        def chunk(p):
+            gain = norm_gain[l:l + 1, lanes(p)]
+
+            def body(i):
+                v = buf[p, i:i + BLK, :].astype(jnp.float32)
+                sq = v * v
+                ss[i:i + BLK, :] = ss[i:i + BLK, :] + (sq[:, 0:128] + sq[:, 128:256])
+                u[i:i + BLK, lanes(p)] = (v * gain).astype(jnp.bfloat16)
+            blocks(rows, body)
+        each(k, chunk)
+
+    def clear_squares(rows):
+        ss[0:rows, :] = jnp.zeros((rows, 128), jnp.float32)
+
+    def factors(rows):
         def body(i):
-            acc[pl.ds(i, BLK), :] = jnp.zeros((BLK, 2 * C), jnp.float32)
+            total = jnp.sum(ss[i:i + BLK, :], axis=1, keepdims=True)
+            ss[i:i + BLK, :] = jnp.broadcast_to(lax.rsqrt(total * (1.0 / d_model) + EPSILON), (BLK, 128))
         blocks(rows, body)
 
-    def prepare(l, buf, rows, lo, hi):
-        def run(j, carry):
-            p = rel(j)
-            gain = norm_gain[l, p]
-
-            def body(i):
-                v = buf[p, pl.ds(i, BLK), :].astype(jnp.float32)
-                sq = v * v
-                part = sq[:, 0:128] + sq[:, 128:256]
-                ss[pl.ds(i, BLK), :] = ss[pl.ds(i, BLK), :] + part
-                u[j, pl.ds(i, BLK), :] = (v * gain).astype(jnp.bfloat16)
-            blocks(rows, body)
-            return carry
-        lax.fori_loop(lo, hi, run, 0)
-
-    def clear_squares(rows):
+    def gate(rows, margin):
+        first = sp * tokens - margin
+        row = lax.broadcasted_iota(jnp.int32, (BLK, 128), 0)
+
         def body(i):
-            ss[pl.ds(i, BLK), :] = jnp.zeros((BLK, 128), jnp.float32)
-        blocks(rows, body)
-
-    def gate(rows, margin):
-        def body(i):
-            total = jnp.sum(ss[pl.ds(i, BLK), :], axis=1, keepdims=True)
-            factor = lax.rsqrt(total * (1.0 / d_model) + EPSILON)
-            at = sp * tokens - margin + i + lax.broadcasted_iota(jnp.int32, (BLK, 128), 0)
+            factor = ss[i:i + BLK, :]
+            at = first + i + row
             inside = (at >= 0) & (at < tokens * sp_n)
             for h in range(2):
-                lin = acc[pl.ds(i, BLK), 256 * h:256 * h + 128] * factor
-                gat = acc[pl.ds(i, BLK), 256 * h + 128:256 * h + 256] * factor
-                val = jnp.where(inside, lin * jax.nn.sigmoid(gat), 0.0)
-                gs[h, pl.ds(i, BLK), :] = val.astype(jnp.bfloat16).astype(jnp.float32)
+                lin = acc[i:i + BLK, 256 * h:256 * h + 128] * factor
+                gat = acc[i:i + BLK, 256 * h + 128:256 * h + 256] * factor
+                val = lin * (0.5 + 0.5 * jnp.tanh(0.5 * gat))
+                val = jnp.where(inside, val, 0.0)
+                gs[h, i:i + BLK, :] = val.astype(jnp.bfloat16).astype(jnp.float32)
         blocks(rows, body)
 
     def convolve(l, buf, rows):
@@ -283,21 +294,22 @@
             sums = []
             for h in range(2):
                 cols = slice(128 * h, 128 * h + 128)
-                total = jnp.broadcast_to(conv_b[l, :, cols], (BLK, 128))
+                total = jnp.broadcast_to(conv_b[l:l + 1, cols], (BLK, 128))
                 for k in range(width):
-                    total = total + gs[h, pl.ds(i + (1 + k), BLK), :] * conv_w[l, k:k + 1, cols]
+                    total = total + gs[h, i + 1 + k:i + 1 + k + BLK, :] * conv_w[k, l:l + 1, cols]
                 sums.append(total)
             mean = jnp.sum(sums[0] + sums[1], axis=1, keepdims=True) * (1.0 / C)
             low, high = sums[0] - mean, sums[1] - mean
             spread = jnp.sum(low * low + high * high, axis=1, keepdims=True)
-            buf[me, pl.ds(i, BLK), 0:128] = low.astype(jnp.bfloat16)
-            buf[me, pl.ds(i, BLK), 128:256] = high.astype(jnp.bfloat16)
-            st[pl.ds(i, BLK), :] = jnp.where(lane == 0, mean, jnp.where(lane == 1, spread, 0.0))
+            buf[me, i:i + BLK, 0:128] = low.astype(jnp.bfloat16)
+            buf[me, i:i + BLK, 128:256] = high.astype(jnp.bfloat16)
+            st[i:i + BLK, :] = jnp.where(lane == 0, mean, jnp.where(lane == 1, spread, 0.0))
         blocks(rows, body)
 
     def stats_send(l):
-        so[l] = st[...].T[0:8, :]
-        sb[l, me] = so[l]
+        both = st[...].T[0:2, :]
+        so[l] = both
+        sb[l, me] = both
         for p in peers:
             remote(so.at[l], sb.at[l, me], st_s.at[l], st_r.at[l], (sp, p)).start()
 
@@ -305,36 +317,51 @@
         whole = sb.at[l, pl.ds(0, tp - 1)]
         return remote(whole, whole, st_s.at[l], st_r.at[l], (sp, sib))
 
-    def stats_take(l):
+    def stats_take(l, rows):
         stats_all(l).wait_recv()
-        means = [sb[l, rel(j), 0:1, :] for j in range(tp)]
-        spreads = [sb[l, rel(j), 1:2, :] for j in range(tp)]
+        means = [sb[l, p, 0:1, :] for p in range(tp)]
+        spreads = [sb[l, p, 1:2, :] for p in range(tp)]
         average = sum(means) * (1.0 / tp)
         apart = [m - average for m in means]
         variance = sum(spreads) * (1.0 / d_model) + sum(v * v for v in apart) * (1.0 / tp)
-        q[0:tp, :] = jnp.concatenate(apart, axis=0)
-        q[tp:tp + 8, :] = jnp.broadcast_to(lax.rsqrt(variance + EPSILON), (8, q.shape[1]))
+        scale = lax.rsqrt(variance + EPSILON)
+        wide = q.shape[1]
+        q[0:8, :] = jnp.broadcast_to(scale, (8, wide))
+        for p in range(tp):
+            q[8 + 8 * p:16 + 8 * p, :] = jnp.broadcast_to(apart[p] * scale, (8, wide))
         qt[...] = q[...].T
-
-    def mix(l, buf, rows, js):
-        for j in js:
-            p = rel(j)
-            gain = lnb[p, l:l + 1, :]
-            shift = lnb[p, 2 + l:3 + l, :]
+        for i in range(0, rows, BLK):
+            ss[i:i + BLK, :] = jnp.broadcast_to(qt[i:i + BLK, 0:1], (BLK, 128))
+
+    def mix(l, buf, rows, k):
+        lane = lax.broadcasted_iota(jnp.int32, (BLK, 128), 1)
+
+        def chunk(p):
+            gain = lnb[p, l:l + 1, :] * 0.5
+            shift = lnb[p, 2 + l:3 + l, :] * 0.5
+            pick = lane == 8 + 8 * p
 
             def body(i):
-                v = buf[p, pl.ds(i, BLK), :].astype(jnp.float32)
-                v = (v + qt[pl.ds(i, BLK), j:j + 1]) * qt[pl.ds(i, BLK), tp:tp + 1] * gain + shift
-                u[j, pl.ds(i, BLK), :] = (v * jax.nn.sigmoid(v)).astype(jnp.bfloat16)
+                moved = jnp.sum(jnp.where(pick, qt[i:i + BLK, :], 0.0), axis=1, keepdims=True)
+                scale = ss[i:i + BLK, :]
+                for h in range(2):
+                    cols = slice(128 * h, 128 * h + 128)
+                    v = buf[p, i:i + BLK, cols].astype(jnp.float32)
+                    v = (v * scale + moved) * gain[:, cols] + shift[:, cols]
+                    at = pl.ds(pl.multiple_of(p * C + 128 * h, 128), 128)
+                    u[i:i + BLK, at] = (v + v * jnp.tanh(v)).astype(jnp.bfloat16)
             blocks(rows, body)
+        each(k, chunk)
 
     def finish(src, rows, skip, dst):
         def body(i):
-            old = src[me, pl.ds(pl.multiple_of(i + skip, 16), BLK), :].astype(jnp.float32)
-            dst[pl.ds(i, BLK), :] = (old + acc[pl.ds(i, BLK), 0:C]).astype(jnp.bfloat16)
+            old = src[me, i + skip:i + skip + BLK, :].astype(jnp.float32)
+            dst[i:i + BLK, :] = (old + acc[i:i + BLK, 0:C]).astype(jnp.bfloat16)
         blocks(rows, body)
 
-    near = min(6, tp)
+    near = range(1, min(3, nx))
+    far = range(3, nx)
+    last = range(2, nx // 2 + 1)
 
     halo = [
         remote(xb0.at[me, pl.ds(HALO, HALO)], xb0.at[me, pl.ds(HALO + tokens, HALO)],
@@ -348,99 +375,107 @@
     for p in peers:
         remote(lno, lnb.at[me], ln_s.at[0], ln_r.at[0], (sp, p)).start()
     ln_all = remote(lnb.at[pl.ds(0, tp - 1)], lnb.at[pl.ds(0, tp - 1)], ln_s.at[0], ln_r.at[0], (sp, sib))
-    clear(r0)
     clear_squares(r0)
     for c in halo:
         c.wait_recv()
     gather_start(0, xb0, r0)
-    first_send(1)
-    prepare(0, xb0, r0, 0, 1)
     first_wait(0)
     ring(0, 0)
-    first_send(2)
+    first_send(1)
+    own_copy(0, xb0, r0).wait_recv()
+    prepare(0, xb0, r0, 0)
+    ring(0, 1)
     gather_hop(0, xb0, r0, 1)
     first_wait(1)
     ring(1, 0)
-    ring(0, 1)
-    first_send(3)
-    own_copy(0, xb0, r0).wait_recv()
     gather_pair(0, xb0, r0, 1)
-    prepare(0, xb0, r0, 1, near)
     ring(0, 2)
-    for hop in range(2, nx // 2 + 1):
+    for k in near:
+        prepare(0, xb0, r0, k)
+    ring(0, 3)
+    for hop in last:
         gather_hop(0, xb0, r0, hop)
         gather_pair(0, xb0, r0, hop)
-    prepare(0, xb0, r0, near, tp)
-    ring(0, 3)
+    for k in far:
+        prepare(0, xb0, r0, k)
+    factors(r0)
     ring(1, 1)
+    first_send(2)
+    ring(0, 4)
+    matmul_whole(0, wag, r0)
+    ring(1, 2)
+    gate(r0, HALO)
     first_wait(2)
     ring(2, 0)
-    ring(0, 4)
-    matmul(0, wag, r0, 0, tp)
-    ring(1, 2)
-    gate(r0, HALO)
-    ring(2, 1)
     convolve(0, mb0, r1)
     stats_send(0)
     gather_start(1, mb0, r1)
     ring(1, 3)
+    first_send(3)
+    ring(2, 1)
+    ln_all.wait_recv()
+    stats_take(0, r1)
     ring(1, 4)
+    own_copy(1, mb0, r1).wait_recv()
+    mix(0, mb0, r1, 0)
+    matmul(0, wo, r1, [0])
+    gather_hop(1, mb0, r1, 1)
+    ring(2, 2)
+    gather_pair(1, mb0, r1, 1)
+    for k in near:
+        mix(0, mb0, r1, k)
+    matmul(0, wo, r1, near)
     first_wait(3)
     ring(3, 0)
-    ring(2, 2)
-    clear(r1)
-    ln_all.wait_recv()
-    stats_take(0)
-    mix(0, mb0, r1, [0])
-    gather_hop(1, mb0, r1, 1)
-    ring(2, 3)
-    own_copy(1, mb0, r1).wait_recv()
-    gather_pair(1, mb0, r1, 1)
-    mix(0, mb0, r1, range(1, near))
-    matmul(0, wo, r1, 0, near)
-    for hop in range(2, nx // 2 + 1):
+    for hop in last:
         gather_hop(1, mb0, r1, hop)
         gather_pair(1, mb0, r1, hop)
-    mix(0, mb0, r1, range(near, tp))
-    matmul(0, wo, r1, near, tp)
+    for k in far:
+        mix(0, mb0, r1, k)
+    matmul(0, wo, r1, far)
     finish(xb0, r1, 16, xb1.at[me])
     gather_start(2, xb1, r1)
+    ring(2, 3)
+    clear_squares(r1)
     ring(2, 4)
+    own_copy(2, xb1, r1).wait_recv()
+    prepare(1, xb1, r1, 0)
+    matmul(1, wag, r1, [0])
     ring(3, 1)
-    clear(r1)
-    clear_squares(r1)
-    prepare(1, xb1, r1, 0, 1)
-    matmul(1, wag, r1, 0, 1)
+    gather_hop(2, xb1, r1, 1)
+    gather_pair(2, xb1, r1, 1)
+    for k in near:
+        prepare(1, xb1, r1, k)
+    matmul(1, wag, r1, near)
     ring(3, 2)
-    gather_hop(2, xb1, r1, 1)
-    ring(3, 3)
-    own_copy(2, xb1, r1).wait_recv()
-    gather_pair(2, xb1, r1, 1)
-    prepare(1, xb1, r1, 1, near)
-    matmul(1, wag, r1, 1, near)
-    for hop in range(2, nx // 2 + 1):
+    for hop in last:
         gather_hop(2, xb1, r1, hop)
         gather_pair(2, xb1, r1, hop)
-    prepare(1, xb1, r1, near, tp)
-    matmul(1, wag, r1, near, tp)
+    for k in far:
+        prepare(1, xb1, r1, k)
+    matmul(1, wag, r1, far)
+    factors(r1)
     gate(r1, HALO // 2)
+    ring(3, 3)
     convolve(1, mb1, r2)
     stats_send(1)
     gather_start(3, mb1, r2)
     ring(3, 4)
-    clear(r2)
-    stats_take(1)
-    mix(1, mb1, r2, [0])
+    stats_take(1, r2)
+    own_copy(3, mb1, r2).wait_recv()
+    mix(1, mb1, r2, 0)
+    matmul(1, wo, r2, [0])
     gather_hop(3, mb1, r2, 1)
-    own_copy(3, mb1, r2).wait_recv()
     gather_pair(3, mb1, r2, 1)
-    mix(1, mb1, r2, range(1, near))
-    matmul(1, wo, r2, 0, near)
-    for hop in range(2, nx // 2 + 1):
+    for k in near:
+        mix(1, mb1, r2, k)
+    matmul(1, wo, r2, near)
+    for hop in last:
         gather_hop(3, mb1, r2, hop)
         gather_pair(3, mb1, r2, hop)
-    mix(1, mb1, r2, range(near, tp))
-    matmul(1, wo, r2, near, tp)
+    for k in far:
+        mix(1, mb1, r2, k)
+    matmul(1, wo, r2, far)
     finish(xb1, r2, 16, out)
 
     ring_drain()
@@ -484,13 +519,13 @@
                 pltpu.VMEM((tp, r1, C), b16),
                 pltpu.VMEM((tp, r1, C), b16),
                 pltpu.VMEM((tp, r2, C), b16),
-                pltpu.VMEM((tp, r0, C), b16),
+                pltpu.VMEM((r0, tp * C), b16),
                 pltpu.VMEM((2, r0 + BLK, 128), f32),
                 pltpu.VMEM((r0, 2 * C), f32),
                 pltpu.VMEM((r0, 128), f32),
                 pltpu.VMEM((lanes, 128), f32),
-                pltpu.VMEM((2, 8, lanes), f32),
-                pltpu.VMEM((2, tp, 8, lanes), f32),
+                pltpu.VMEM((2, 2, lanes), f32),
+                pltpu.VMEM((2, tp, 2, lanes), f32),
                 pltpu.VMEM((128, lanes), f32),
                 pltpu.VMEM((lanes, 128), f32),
                 pltpu.VMEM((8, C), f32),
@@ -509,8 +544,7 @@
                 collective_id=0, has_side_effects=True, vmem_limit_bytes=56 * 1024 * 1024
             ),
         )(
-            stream, a_w, g_w, o_w, norm_gain.reshape(2, tp, 1, C), conv_w,
-            conv_b.reshape(2, 1, C), ln_gain, ln_shift,
+            stream, a_w, g_w, o_w, norm_gain, jnp.transpose(conv_w, (1, 0, 2)), conv_b, ln_gain, ln_shift,
         )
 
     return jax.shard_map(local, mesh=mesh, in_specs=spec, out_specs=P("sp", "tp"), check_vma=False)

time: 119 us -> 92.1 us (0.77)
  Pallas kernels: 113 us -> 90.3 us
  local copies, waits for them, and re-layouts: 5.67 us -> 1.62 us
    pallas_call x1, Pallas kernels: 113 us -> 90.3 us  [local(): pl.pallas_call(functools.partial(kernel, nz, ny, nx, tokens, width), out_...]
    reshape x2 -> x0, local copies, waits for them, and re-layouts: 2.59 us -> none  [the longest x1 1.35 us: local(): norm_gain.reshape(2, tp, 1, C)]
    unnamed x2 -> x1, local copies, waits for them, and re-layouts: 3.08 us -> 1.62 us
where the time goes in v2:
time: 92.1 us; the launch traced here: 91.9 us
  Pallas kernels  90.3 us (98%)
  local copies, waits for them, and re-layouts  1.62 us (2%)
    pallas_call x1, Pallas kernels, local(): pl.pallas_call(functools.partial(kernel, nz, ny, nx, tokens, width), out_...  90.3 us

profile of v2, /device:TPU:1, one launch (start us, length us, event | category | flops | bytes accessed | tf_op | source)
XLA Modules:
  0.0 91.9 jit_solution(9185227319136522486)
XLA Ops:
  0.0 90.3 %shard_map.91 = bf16[384,256]{1,0:T(8,128)(2,1)} custom-call(bf16[384,256]{1,0:T(8,128)(2,1)} %stream.1, bf16[2,32,256]{2,1,0:T(8,128)(2,1)} %a_w.1, bf16[2,32,256]{2,1,0:T(8,128)(2,1)} %g_w.1, bf16[2,32,256]{2,1,0:T(8,128)(2,1)} %o_w.1, f32[2,2048]{1,0:T(2,128)} %norm_gain.1, f32[31,2,256]{2,1,0:T(2,128)} %bitcast.1, f32[2,256]{1,0:T(2,128)} %conv_b.1, ...), custom_call_target="tpu_custom_call" | custom-call | tf_op jit(solution)/shard_map/pallas_call | solution.py:510
  90.3 1.6 %copy.11 = bf16[384,256]{1,0:T(8,128)(2,1)} copy(bf16[384,256]{1,0:T(8,128)(2,1)} %shard_map.91) | data formatting | bytes 393216

commit v3 on v2

v3 whole, which is shorter than its diff:
```python
import functools

import jax
import jax.numpy as jnp
from jax import lax
from jax.experimental import pallas as pl
from jax.experimental.pallas import tpu as pltpu
from jax.sharding import PartitionSpec as P

EPSILON = 1e-06
MESH = pl.DeviceIdType.MESH
C = 256
HALO = 32
BLK = 32
SUB = (4, 2, 4, 1)
ITEMS = [(st, h) for st in range(4) for h in range(SUB[st])]


def remote(src, dst, ssem, rsem, dev):
    return pltpu.make_async_remote_copy(
        src_ref=src, dst_ref=dst, send_sem=ssem, recv_sem=rsem, device_id=dev, device_id_type=MESH
    )


def kernel(
    nz, ny, nx, tokens, width,
    stream, a_w, g_w, o_w, norm_gain_in, conv_w_in, conv_b_in, ln_gain_in, ln_shift_in,
    out,
    norm_gain, conv_w, conv_b, ln_gain, ln_shift, outv, wag, wo, xb0, xb1, mb0, mb1, u, gs, acc, ss, sc, st, so, sb, q, qt, lno, lnb,
    p1_s, p1_r, po_r, rg_s, rg_r, xg_s, xg_r, dd_r, do_r, hl_s, hl_r, st_s, st_r, ln_s, ln_r, loc,
):
    tp = 2 * nx
    sp_n = nz * ny
    d_model = C * tp
    kb = d_model // sp_n
    sp = lax.axis_index("sp")
    me = lax.axis_index("tp")
    z, y = sp // ny, lax.rem(sp, ny)
    x, core = me // 2, lax.rem(me, 2)
    sib = me + 1 - 2 * core
    r0, r1, r2 = tokens + 2 * HALO, tokens + HALO, tokens
    cut = (r1 // 2 + BLK - 1) // BLK * BLK

    def spid(zz, yy):
        return lax.rem(zz, nz) * ny + lax.rem(yy, ny)

    peers = [lax.rem(me + j, tp) for j in range(1, tp)]
    nxt, prv = lax.rem(sp + 1, sp_n), lax.rem(sp + sp_n - 1, sp_n)

    barrier = pltpu.get_barrier_semaphore()

    def greet(dev):
        pl.semaphore_signal(barrier, inc=1, device_id=dev, device_id_type=MESH)

    for j in range(1, ny):
        greet((spid(z, y + j), me))
    for j in range(1, nz):
        greet((spid(z + j, y), me))
    greet((nxt, me))
    greet((prv, me))
    for p in peers:
        greet((sp, p))

    local = [pltpu.make_async_copy(stream, xb0.at[me, pl.ds(HALO, tokens)], loc.at[0]),
             pltpu.make_async_copy(o_w, wo.at[:, z, y], loc.at[1])]
    for l in range(2):
        for h in range(2):
            src = pl.ds(128 * h, 128)
            pltpu.make_async_copy(
                a_w.at[l, :, src], wag.at[l, z, y, :, pl.ds(256 * h, 128)], loc.at[2]).start()
            pltpu.make_async_copy(
                g_w.at[l, :, src], wag.at[l, z, y, :, pl.ds(256 * h + 128, 128)], loc.at[2]).start()
    pairs = pltpu.make_async_copy(wag.at[:, z, y], wag.at[:, z, y], loc.at[2])
    n = 3
    small = [pltpu.make_async_copy(src, dst, loc.at[n + i]) for i, (src, dst) in enumerate((
        (ln_gain_in, ln_gain), (ln_shift_in, ln_shift), (norm_gain_in, norm_gain),
        (conv_w_in, conv_w), (conv_b_in, conv_b)))]
    for c in local + small:
        c.start()
    for c in small[0:2]:
        c.wait()
    lno[...] = jnp.zeros_like(lno)
    lno[0:2, :] = ln_gain[...]
    lno[2:4, :] = ln_shift[...]
    lnb[me] = lno[...]
    for c in local + small[2:]:
        c.wait()
    pairs.wait()
    pl.semaphore_wait(barrier, ny + nz + tp - 1)

    def weight(stage, path):
        buf, cols = (wag, 256) if stage % 2 == 0 else (wo, 128)
        return buf.at[stage // 2], pl.ds(cols * path, cols)

    def first_axis(path):
        return (ny, y) if path == 0 else (nz, z)

    def first_to(path, index):
        return (spid(z, index), me) if path == 0 else (spid(index, y), me)

    def first_some(stage, path, count):
        ref, cols = weight(stage, path)
        if path == 0:
            return ref.at[0, pl.ds(0, count), :, cols]
        return ref.at[pl.ds(0, count), 0, :, cols]

    def first_send(stage):
        reach = [0, 0]
        for path in range(2):
            size, at = first_axis(path)
            reach[path] = [j for d in range(1, size // 2 + 1) for j in sorted({d, size - d})]
        for i in range(max(len(r) for r in reach)):
            for path in range(2):
                size, at = first_axis(path)
                if i >= len(reach[path]):
                    continue
                ref, cols = weight(stage, path)
                mine = ref.at[z, y, :, cols]
                to = lax.rem(at + reach[path][i], size)
                part = size // SUB[0]
                slot = lax.rem(at // part - to // part + SUB[0], SUB[0])
                arrived = p1_r.at[path, slot] if stage == 0 else po_r.at[path, stage - 1]
                remote(mine, mine, p1_s.at[stage], arrived, first_to(path, to)).start()

    def first_wait(slot):
        for path in range(2):
            size, _ = first_axis(path)
            count = size // SUB[0] - (1 if slot == 0 else 0)
            if count:
                whole = first_some(0, path, count)
                remote(whole, whole, p1_s.at[0], p1_r.at[path, slot], (sp, sib)).wait_recv()

    def first_rest(stage):
        for path in range(2):
            whole = first_some(stage, path, first_axis(path)[0] - 1)
            remote(whole, whole, p1_s.at[stage], po_r.at[path, stage - 1], (sp, sib)).wait_recv()

    def ring_block(item, path, origin):
        stage, h = ITEMS[item]
        ref, cols = weight(stage, path)
        if stage == 0:
            size, at = first_axis(path)
            h = lax.rem(at // (size // SUB[0]) + h, SUB[0])
        if path == 0:
            m = ny // SUB[stage]
            return ref.at[origin, pl.ds(h * m, m), :, cols]
        m = nz // SUB[stage]
        return ref.at[pl.ds(h * m, m), origin, :, cols]

    def ring_hops(item, path, way):
        size = nz if path == 0 else ny
        return size // 2 if (item + way) % 2 == 0 else size - 1 - size // 2

    def ring_copy(item, path, way, hop, origin, far=1):
        step = far if way == 0 else -far
        if path == 0:
            to = spid(z + nz + step, y)
        else:
            to = spid(z, y + ny + step)
        block = ring_block(item, path, origin)
        base = 0 if way == 0 else ring_hops(item, path, 0)
        return remote(block, block, rg_s.at[ITEMS[item][0] % 2], rg_r.at[path, item, base + hop], (to, me))

    def ring(stage, hop, only=None):
        order = [i for i, (of, _) in enumerate(ITEMS) if of == stage]
        if stage == 0:
            order = [0, 1, 3, 2]
        for item in order if only is None else only:
            for path in range(2):
                size, at = (nz, z) if path == 0 else (ny, y)
                for way in range(2):
                    hops = ring_hops(item, path, way)
                    jump = hops == size // 2 and hops >= 2
                    step = 1 if way == 0 else -1
                    origin = lax.rem(at + 2 * size - step * hop, size)
                    if 0 < hop <= hops:
                        ring_copy(item, path, way, hop - 1, origin).wait_recv()
                    if hop < hops - (1 if jump else 0):
                        ring_copy(item, path, way, hop, origin).start()
                    if jump and hop == hops - 2:
                        ring_copy(item, path, way, hops - 1, origin, 2).start()

    def ring_drain():
        for ref, sem in (
            (wag.at[:, pl.ds(0, nz - 1)], rg_s.at[0]), (wo.at[:, pl.ds(0, nz - 1)], rg_s.at[1]),
            (wag.at[0, 0, pl.ds(0, ny - 1)], p1_s.at[0]), (wo.at[0, 0, pl.ds(0, ny - 1)], p1_s.at[3]),
            (wo.at[0, 0, pl.ds(0, ny - 1)], p1_s.at[1]), (wag.at[0, 0, pl.ds(0, ny - 1)], p1_s.at[2]),
        ):
            remote(ref, ref, sem, sem, (sp, sib)).wait_send()

    def x_hops(half, way):
        return nx // 2 if (half + way) % 2 == 0 else nx - 1 - nx // 2

    def x_order(way):
        return (0, 1) if way == 0 else (1, 0)

    def span(g):
        if g == 0:
            return xb0, 0, r0
        buf = (mb0, xb1, mb1)[(g - 1) // 2]
        top = (cut, cut, cut - HALO)[(g - 1) // 2]
        rows = (r1, r1, r2)[(g - 1) // 2]
        return (buf, 0, top) if g % 2 == 1 else (buf, top, rows - top)

    def x_piece(g, half, owner):
        buf, lo, rows = span(g)
        mid = (rows // 2 + 15) // 16 * 16
        return buf.at[owner, pl.ds(lo, mid) if half == 0 else pl.ds(lo + mid, rows - mid)]

    def x_owner(way, hop):
        step = 1 if way == 0 else -1
        return lax.rem(x + 2 * nx - step * hop, nx) * 2 + core

    def x_pieces(hop):
        return [(half, way) for k in range(2) for way in range(2)
                for half in (x_order(way)[k],) if hop <= x_hops(half, way)]

    def x_index(half, way, hop):
        flat = [(hp, p) for hp in range(1, nx // 2 + 1) for p in x_pieces(hp)]
        return flat.index((hop, (half, way)))

    def x_copy(g, half, way, hop):
        step = 1 if way == 0 else -1
        to = lax.rem(x + nx + step, nx) * 2 + core
        piece = x_piece(g, half, x_owner(way, hop))
        return remote(piece, piece, xg_s.at[g], xg_r.at[g, x_index(half, way, hop + 1)], (sp, to))

    def d_copy(g, half, way, hop):
        piece = x_piece(g, half, x_owner(way, hop))
        return remote(piece, piece, xg_s.at[g], dd_r.at[g, hop - 1], (sp, sib))

    def own_copy(g):
        buf, lo, rows = span(g)
        piece = buf.at[me, pl.ds(lo, rows)]
        return remote(piece, piece, xg_s.at[g], do_r.at[g], (sp, sib))

    def some(pieces, part):
        return pieces if part is None else pieces[2 * part:2 * part + 2]

    def gather_start(g, part=None):
        for half, way in some(x_pieces(1), part):
            x_copy(g, half, way, 0).start()
        if part != 1:
            own_copy(g).start()

    def gather_hop(g, hop, part=None):
        for half, way in some(x_pieces(hop), part):
            x_copy(g, half, way, hop - 1).wait_recv()
            if hop < x_hops(half, way):
                x_copy(g, half, way, hop).start()
            d_copy(g, half, way, hop).start()

    def gather_pair(g, hop):
        buf, lo, rows = span(g)
        whole = buf.at[pl.ds(0, len(x_pieces(hop)) // 2), pl.ds(lo, rows)]
        remote(whole, whole, xg_s.at[g], dd_r.at[g, hop - 1], (sp, sib)).wait_recv()

    def gather_drain(g):
        buf, lo, rows = span(g)
        whole = buf.at[pl.ds(0, tp - 1), pl.ds(lo, rows)]
        remote(whole, whole, xg_s.at[g], do_r.at[g], (sp, sib)).wait_send()

    def blocks(rng, body):
        for i in range(rng[0], rng[0] + rng[1], BLK):
            body(i)

    def pair_chip(k):
        return lax.rem(x + (0, nx - 1, 1, 2)[k], nx)

    def each(k, body):
        def run(c, carry):
            body(pair_chip(k) * 2 + c)
            return carry
        lax.fori_loop(0, 2, run, 0)

    def lanes(p):
        return pl.ds(pl.multiple_of(p * C, C), C)

    def matmul(l, ref, rng, ks):
        cols = ref.shape[-1]
        rows = slice(rng[0], rng[0] + rng[1])
        for k in ks:
            chip = pair_chip(k)
            left = u[rows, pl.ds(pl.multiple_of(chip * 2 * C, 2 * C), 2 * C)]
            right = ref[l, pl.ds(chip * 2, 2)].reshape(2 * C, cols)
            part = jnp.dot(left, right, preferred_element_type=jnp.float32)
            if k == 0:
                acc[rows, 0:cols] = part
            else:
                acc[rows, 0:cols] = acc[rows, 0:cols] + part

    def matmul_whole(l, ref, rng):
        cols = ref.shape[-1]
        rows = slice(rng[0], rng[0] + rng[1])
        for h in range(cols // C):
            right = ref[l, :, :, :, C * h:C * h + C].reshape(d_model, C)
            acc[rows, C * h:C * h + C] = jnp.dot(u[rows, :], right, preferred_element_type=jnp.float32)

    def prepare(l, buf, rng, k):
        def chunk(p):
            gain = norm_gain[l:l + 1, lanes(p)]

            def body(i):
                v = buf[p, i:i + BLK, :].astype(jnp.float32)
                sq = v * v
                ss[i:i + BLK, :] = ss[i:i + BLK, :] + (sq[:, 0:128] + sq[:, 128:256])
                u[i:i + BLK, lanes(p)] = (v * gain).astype(jnp.bfloat16)
            blocks(rng, body)
        each(k, chunk)

    def clear_squares(rng):
        ss[rng[0]:rng[0] + rng[1], :] = jnp.zeros((rng[1], 128), jnp.float32)

    def factors(rng):
        def body(i):
            total = jnp.sum(ss[i:i + BLK, :], axis=1, keepdims=True)
            ss[i:i + BLK, :] = jnp.broadcast_to(lax.rsqrt(total * (1.0 / d_model) + EPSILON), (BLK, 128))
        blocks(rng, body)

    def gate(rng, margin):
        first = sp * tokens - margin
        row = lax.broadcasted_iota(jnp.int32, (BLK, 128), 0)

        def body(i):
            factor = ss[i:i + BLK, :]
            at = first + i + row
            inside = (at >= 0) & (at < tokens * sp_n)
            for h in range(2):
                lin = acc[i:i + BLK, 256 * h:256 * h + 128] * factor
                gat = acc[i:i + BLK, 256 * h + 128:256 * h + 256] * factor
                val = lin * (0.5 + 0.5 * jnp.tanh(0.5 * gat))
                val = jnp.where(inside, val, 0.0)
                gs[h, i:i + BLK, :] = val.astype(jnp.bfloat16).astype(jnp.float32)
        blocks(rng, body)

    def convolve(l, buf, rng):
        lane = lax.broadcasted_iota(jnp.int32, (BLK, 128), 1)

        def body(i):
            sums = []
            for h in range(2):
                cols = slice(128 * h, 128 * h + 128)
                total = jnp.broadcast_to(conv_b[l:l + 1, cols], (BLK, 128))
                for k in range(width):
                    total = total + gs[h, i + 1 + k:i + 1 + k + BLK, :] * conv_w[k, l:l + 1, cols]
                sums.append(total)
            mean = jnp.sum(sums[0] + sums[1], axis=1, keepdims=True) * (1.0 / C)
            low, high = sums[0] - mean, sums[1] - mean
            spread = jnp.sum(low * low + high * high, axis=1, keepdims=True)
            buf[me, i:i + BLK, 0:128] = low.astype(jnp.bfloat16)
            buf[me, i:i + BLK, 128:256] = high.astype(jnp.bfloat16)
            r = i - rng[0]
            st[r:r + BLK, :] = jnp.where(lane == 0, mean, jnp.where(lane == 1, spread, 0.0))
        blocks(rng, body)

    def stats_send(l, h):
        both = st[...].T[0:2, :]
        so[l, h] = both
        sb[l, h, me] = both
        for p in peers:
            remote(so.at[l, h], sb.at[l, h, me], st_s.at[2 * l + h], st_r.at[2 * l + h], (sp, p)).start()

    def stats_all(l, h):
        whole = sb.at[l, h, pl.ds(0, tp - 1)]
        return remote(whole, whole, st_s.at[2 * l + h], st_r.at[2 * l + h], (sp, sib))

    def stats_take(l, h):
        stats_all(l, h).wait_recv()
        means = [sb[l, h, p, 0:1, :] for p in range(tp)]
        spreads = [sb[l, h, p, 1:2, :] for p in range(tp)]
        average = sum(means) * (1.0 / tp)
        apart = [m - average for m in means]
        variance = sum(spreads) * (1.0 / d_model) + sum(v * v for v in apart) * (1.0 / tp)
        scale = lax.rsqrt(variance + EPSILON)
        wide = q.shape[1]
        q[0:8, :] = jnp.broadcast_to(scale, (8, wide))
        for p in range(tp):
            q[8 + 8 * p:16 + 8 * p, :] = jnp.broadcast_to(apart[p] * scale, (8, wide))
        qt[h] = q[...].T
        for i in range(0, wide, BLK):
            sc[h, i:i + BLK, :] = jnp.broadcast_to(qt[h, i:i + BLK, 0:1], (BLK, 128))

    def mix(l, buf, rng, h, k):
        lane = lax.broadcasted_iota(jnp.int32, (BLK, 128), 1)

        def chunk(p):
            gain = lnb[p, l:l + 1, :] * 0.5
            shift = lnb[p, 2 + l:3 + l, :] * 0.5
            pick = lane == 8 + 8 * p

            def body(i):
                r = i - rng[0]
                moved = jnp.sum(jnp.where(pick, qt[h, r:r + BLK, :], 0.0), axis=1, keepdims=True)
                scale = sc[h, r:r + BLK, :]
                for c in range(2):
                    cols = slice(128 * c, 128 * c + 128)
                    v = buf[p, i:i + BLK, cols].astype(jnp.float32)
                    v = (v * scale + moved) * gain[:, cols] + shift[:, cols]
                    at = pl.ds(pl.multiple_of(p * C + 128 * c, 128), 128)
                    u[i:i + BLK, at] = (v + v * jnp.tanh(v)).astype(jnp.bfloat16)
            blocks(rng, body)
        each(k, chunk)

    def finish(src, rng, skip, dst):
        def body(i):
            old = src[me, i + skip:i + skip + BLK, :].astype(jnp.float32)
            dst[i:i + BLK, :] = (old + acc[i:i + BLK, 0:C]).astype(jnp.bfloat16)
        blocks(rng, body)

    near = range(1, min(3, nx))
    far = range(3, nx)
    last = range(2, nx // 2 + 1)

    halo = [
        remote(xb0.at[me, pl.ds(HALO, HALO)], xb0.at[me, pl.ds(HALO + tokens, HALO)],
               hl_s.at[0], hl_r.at[0], (prv, me)),
        remote(xb0.at[me, pl.ds(tokens, HALO)], xb0.at[me, pl.ds(0, HALO)],
               hl_s.at[1], hl_r.at[1], (nxt, me)),
    ]
    for c in halo:
        c.start()
    first_send(0)
    first_send(1)
    for p in peers:
        remote(lno, lnb.at[me], ln_s.at[0], ln_r.at[0], (sp, p)).start()
    ln_all = remote(lnb.at[pl.ds(0, tp - 1)], lnb.at[pl.ds(0, tp - 1)], ln_s.at[0], ln_r.at[0], (sp, sib))
    clear_squares((0, r0))
    first_wait(0)
    ring(0, 0, [0])
    first_wait(1)
    ring(0, 0, [1])
    for c in halo:
        c.wait_recv()
    gather_start(0)
    first_wait(3)
    ring(0, 0, [3])
    first_wait(2)
    ring(0, 0, [2])
    ring(0, 1)
    first_rest(1)
    ring(1, 0)
    gather_hop(0, 1, 0)
    ring(0, 2)
    gather_hop(0, 1, 1)
    own_copy(0).wait_recv()
    prepare(0, xb0, (0, r0), 0)
    for hop in last:
        gather_hop(0, hop)
    gather_pair(0, 1)
    for k in near:
        prepare(0, xb0, (0, r0), k)
    for hop in last:
        gather_pair(0, hop)
    for k in far:
        prepare(0, xb0, (0, r0), k)
    factors((0, r0))
    ring(1, 1)
    first_send(2)
    ring(0, 3)
    ring(0, 4)
    top, low = (0, cut + HALO), (cut + HALO, r0 - cut - HALO)
    matmul_whole(0, wag, top)
    gate(top, HALO)
    convolve(0, mb0, (0, cut))
    stats_send(0, 0)
    gather_start(1)
    matmul_whole(0, wag, low)
    gate(low, HALO)
    convolve(0, mb0, (cut, r1 - cut))
    stats_send(0, 1)
    gather_start(2, 0)
    top, low = (0, cut), (cut, r1 - cut)
    ln_all.wait_recv()
    ring(1, 2)
    first_rest(2)
    ring(2, 0)
    stats_take(0, 0)
    own_copy(1).wait_recv()
    mix(0, mb0, top, 0, 0)
    gather_hop(1, 1, 0)
    gather_start(2, 1)
    gather_hop(1, 1, 1)
    stats_take(0, 1)
    own_copy(2).wait_recv()
    mix(0, mb0, low, 1, 0)
    gather_hop(2, 1, 0)
    gather_pair(1, 1)
    for k in near:
        mix(0, mb0, top, 0, k)
    for hop in last:
        gather_hop(1, hop)
    gather_hop(2, 1, 1)
    ring(2, 1)
    first_send(3)
    for hop in last:
        gather_pair(1, hop)
    for k in far:
        mix(0, mb0, top, 0, k)
    ring(1, 3)
    ring(1, 4)
    matmul_whole(0, wo, top)
    finish(xb0, top, 16, xb1.at[me])
    gather_start(3)
    for hop in last:
        gather_hop(2, hop)
    gather_pair(2, 1)
    for k in near:
        mix(0, mb0, low, 1, k)
    for hop in last:
        gather_pair(2, hop)
    for k in far:
        mix(0, mb0, low, 1, k)
    matmul_whole(0, wo, low)
    finish(xb0, low, 16, xb1.at[me])
    gather_start(4, 0)
    clear_squares((0, r1))
    own_copy(3).wait_recv()
    prepare(1, xb1, top, 0)
    ring(2, 2)
    gather_hop(3, 1, 0)
    gather_start(4, 1)
    gather_hop(3, 1, 1)
    first_rest(3)
    ring(3, 0)
    own_copy(4).wait_recv()
    prepare(1, xb1, low, 0)
    gather_pair(3, 1)
    for k in near:
        prepare(1, xb1, top, k)
    gather_hop(4, 1, 0)
    for hop in last:
        gather_hop(3, hop)
    gather_hop(4, 1, 1)
    for hop in last:
        gather_pair(3, hop)
    for k in far:
        prepare(1, xb1, top, k)
    ring(2, 3)
    ring(2, 4)
    matmul_whole(1, wag, top)
    factors(top)
    gate(top, HALO // 2)
    convolve(1, mb1, (0, cut - HALO))
    stats_send(1, 0)
    gather_start(5)
    ring(3, 1)
    for hop in last:
        gather_hop(4, hop)
    gather_pair(4, 1)
    for k in near:
        prepare(1, xb1, low, k)
    for hop in last:
        gather_pair(4, hop)
    ring(3, 2)
    for k in far:
        prepare(1, xb1, low, k)
    matmul_whole(1, wag, low)
    factors(low)
    gate(low, HALO // 2)
    top, low = (0, cut - HALO), (cut - HALO, r2 - cut + HALO)
    convolve(1, mb1, low)
    stats_send(1, 1)
    gather_start(6, 0)
    stats_take(1, 0)
    own_copy(5).wait_recv()
    mix(1, mb1, top, 0, 0)
    gather_hop(5, 1, 0)
    gather_start(6, 1)
    gather_hop(5, 1, 1)
    stats_take(1, 1)
    own_copy(6).wait_recv()
    mix(1, mb1, low, 1, 0)
    gather_hop(6, 1, 0)
    gather_pair(5, 1)
    for k in near:
        mix(1, mb1, top, 0, k)
    ring(3, 3)
    ring(3, 4)
    matmul(1, wo, top, [0])
    matmul(1, wo, top, near)
    for hop in last:
        gather_hop(5, hop)
    gather_hop(6, 1, 1)
    for hop in last:
        gather_pair(5, hop)
    for k in far:
        mix(1, mb1, top, 0, k)
    matmul(1, wo, top, far)
    finish(xb1, top, 16, outv)
    result = [pltpu.make_async_copy(outv.at[pl.ds(*rng)], out.at[pl.ds(*rng)], loc.at[i])
              for i, rng in enumerate((top, low))]
    result[0].start()
    for hop in last:
        gather_hop(6, hop)
    gather_pair(6, 1)
    for k in near:
        mix(1, mb1, low, 1, k)
    matmul(1, wo, low, [0])
    matmul(1, wo, low, near)
    for hop in last:
        gather_pair(6, hop)
    for k in far:
        mix(1, mb1, low, 1, k)
    matmul(1, wo, low, far)
    finish(xb1, low, 16, outv)
    result[1].start()

    ring_drain()
    for g in range(7):
        gather_drain(g)
    for c in halo:
        c.wait_send()
    for l in range(2):
        for h in range(2):
            stats_all(l, h).wait_send()
    ln_all.wait_send()
    for c in result:
        c.wait()


def build(mesh, nz, ny, nx):
    tp = 2 * nx
    spec = (
        P("sp", "tp"), P(), P(None, "sp", "tp"), P(None, "sp", "tp"), P(None, None, "tp"),
        P(None, "tp"), P(None, "tp"), P(None, "tp"), P(None, "sp", "tp"),
    )

    def local(stream, norm_gain, a_w, g_w, conv_w, conv_b, ln_gain, ln_shift, o_w):
        tokens = stream.shape[0]
        width = conv_w.shape[1]
        kb = a_w.shape[1]
        r0, r1, r2 = tokens + 2 * HALO, tokens + HALO, tokens
        lanes = ((r1 // 2 + BLK - 1) // BLK * BLK + 127) // 128 * 128
        dma, f32, b16 = pltpu.SemaphoreType.DMA, jnp.float32, jnp.bfloat16
        hops = max(nz, ny) // 2
        anywhere = pl.BlockSpec(memory_space=pl.ANY)
        return pl.pallas_call(
            functools.partial(kernel, nz, ny, nx, tokens, width),
            out_shape=jax.ShapeDtypeStruct((tokens, C), b16),
            in_specs=[anywhere] * 9,
            out_specs=anywhere,
            scratch_shapes=[
                pltpu.VMEM((2, tp * C), f32),
                pltpu.VMEM((width, 2, C), f32),
                pltpu.VMEM((2, C), f32),
                pltpu.VMEM((2, C), f32),
                pltpu.VMEM((2, C), f32),
                pltpu.VMEM((tokens, C), b16),
                pltpu.VMEM((2, nz, ny, kb, 2 * C), b16),
                pltpu.VMEM((2, nz, ny, kb, C), b16),
                pltpu.VMEM((tp, r0, C), b16),
                pltpu.VMEM((tp, r1, C), b16),
                pltpu.VMEM((tp, r1, C), b16),
                pltpu.VMEM((tp, r2, C), b16),
                pltpu.VMEM((r0, tp * C), b16),
                pltpu.VMEM((2, r0 + BLK, 128), f32),
                pltpu.VMEM((r0, 2 * C), f32),
                pltpu.VMEM((r0, 128), f32),
                pltpu.VMEM((2, lanes, 128), f32),
                pltpu.VMEM((lanes, 128), f32),
                pltpu.VMEM((2, 2, 2, lanes), f32),
                pltpu.VMEM((2, 2, tp, 2, lanes), f32),
                pltpu.VMEM((128, lanes), f32),
                pltpu.VMEM((2, lanes, 128), f32),
                pltpu.VMEM((8, C), f32),
                pltpu.VMEM((tp, 8, C), f32),
                dma((4,)), dma((2, SUB[0])), dma((2, 3)),
                dma((2,)), dma((2, len(ITEMS), 2 * hops - 1)),
                dma((7,)), dma((7, 3 * (nx // 2))), dma((7, nx // 2)), dma((7,)),
                dma((2,)), dma((2,)),
                dma((4,)), dma((4,)),
                dma((1,)), dma((1,)),
                dma((8,)),
            ],
            compiler_params=pltpu.CompilerParams(
                collective_id=0, has_side_effects=True, vmem_limit_bytes=56 * 1024 * 1024
            ),
        )(
            stream, a_w, g_w, o_w, norm_gain, jnp.transpose(conv_w, (1, 0, 2)), conv_b, ln_gain, ln_shift,
        )

    return jax.shard_map(local, mesh=mesh, in_specs=spec, out_specs=P("sp", "tp"), check_vma=False)


def solution(mesh):
    return build(mesh, 8, 8, 4)
```

time: 92.1 us -> 79.6 us (0.86)
  Pallas kernels: 90.3 us -> 77.8 us
    pallas_call x1, Pallas kernels: 90.3 us -> 77.8 us  [local(): pl.pallas_call(functools.partial(kernel, nz, ny, nx, tokens, width), out_...]
where the time goes in v3:
time: 79.6 us; the launch traced here: 79.5 us
  Pallas kernels  77.8 us (98%)
  local copies, waits for them, and re-layouts  1.62 us (2%)
    pallas_call x1, Pallas kernels, local(): pl.pallas_call(functools.partial(kernel, nz, ny, nx, tokens, width), out_...  77.8 us
    unnamed x1, local copies, waits for them, and re-layouts  1.62 us

profile of v3, /device:TPU:1, one launch (start us, length us, event | category | flops | bytes accessed | tf_op | source)
XLA Modules:
  0.0 79.5 jit_solution(2644839436397899014)
XLA Ops:
  0.0 77.8 %shard_map.91 = bf16[384,256]{1,0:T(8,128)(2,1)} custom-call(bf16[384,256]{1,0:T(8,128)(2,1)} %stream.1, bf16[2,32,256]{2,1,0:T(8,128)(2,1)} %a_w.1, bf16[2,32,256]{2,1,0:T(8,128)(2,1)} %g_w.1, bf16[2,32,256]{2,1,0:T(8,128)(2,1)} %o_w.1, f32[2,2048]{1,0:T(2,128)} %norm_gain_in.1, f32[31,2,256]{2,1,0:T(2,128)} %bitcast.1, f32[2,256]{1,0:T(2,128)} %conv_b_in.1, ...), custom_call_target="tpu_custom_call" | custom-call | tf_op jit(solution)/shard_map/pallas_call | solution.py:637
  77.8 1.6 %copy.11 = bf16[384,256]{1,0:T(8,128)(2,1)} copy(bf16[384,256]{1,0:T(8,128)(2,1)} %shard_map.91) | data formatting | bytes 393216

commit v4 on v3

--- a/solution.py
+++ b/solution.py
@@ -26,7 +26,7 @@
     nz, ny, nx, tokens, width,
     stream, a_w, g_w, o_w, norm_gain_in, conv_w_in, conv_b_in, ln_gain_in, ln_shift_in,
     out,
-    norm_gain, conv_w, conv_b, ln_gain, ln_shift, outv, wag, wo, xb0, xb1, mb0, mb1, u, gs, acc, ss, sc, st, so, sb, q, qt, lno, lnb,
+    norm_gain, conv_w, conv_b, ln_gain, ln_shift, wag, wo, xb0, xb1, mb0, mb1, u, gs, acc, ss, sc, st, so, sb, q, qt, lno, lnb,
     p1_s, p1_r, po_r, rg_s, rg_r, xg_s, xg_r, dd_r, do_r, hl_s, hl_r, st_s, st_r, ln_s, ln_r, loc,
 ):
     tp = 2 * nx
@@ -472,13 +472,19 @@
     top, low = (0, cut), (cut, r1 - cut)
     ln_all.wait_recv()
     ring(1, 2)
+
+    def pass_on():
+        gather_hop(1, 1, 0)
+        gather_start(2, 1)
+
+    pl.when(core == 1)(pass_on)
     first_rest(2)
     ring(2, 0)
     stats_take(0, 0)
+    first_send(3)
     own_copy(1).wait_recv()
     mix(0, mb0, top, 0, 0)
-    gather_hop(1, 1, 0)
-    gather_start(2, 1)
+    pl.when(core == 0)(pass_on)
     gather_hop(1, 1, 1)
     stats_take(0, 1)
     own_copy(2).wait_recv()
@@ -491,7 +497,6 @@
         gather_hop(1, hop)
     gather_hop(2, 1, 1)
     ring(2, 1)
-    first_send(3)
     for hop in last:
         gather_pair(1, hop)
     for k in far:
@@ -506,6 +511,8 @@
     gather_pair(2, 1)
     for k in near:
         mix(0, mb0, low, 1, k)
+    first_rest(3)
+    ring(3, 0)
     for hop in last:
         gather_pair(2, hop)
     for k in far:
@@ -520,8 +527,7 @@
     gather_hop(3, 1, 0)
     gather_start(4, 1)
     gather_hop(3, 1, 1)
-    first_rest(3)
-    ring(3, 0)
+    ring(3, 1)
     own_copy(4).wait_recv()
     prepare(1, xb1, low, 0)
     gather_pair(3, 1)
@@ -543,7 +549,7 @@
     convolve(1, mb1, (0, cut - HALO))
     stats_send(1, 0)
     gather_start(5)
-    ring(3, 1)
+    ring(3, 2)
     for hop in last:
         gather_hop(4, hop)
     gather_pair(4, 1)
@@ -551,7 +557,6 @@
         prepare(1, xb1, low, k)
     for hop in last:
         gather_pair(4, hop)
-    ring(3, 2)
     for k in far:
         prepare(1, xb1, low, k)
     matmul_whole(1, wag, low)
@@ -586,10 +591,7 @@
     for k in far:
         mix(1, mb1, top, 0, k)
     matmul(1, wo, top, far)
-    finish(xb1, top, 16, outv)
-    result = [pltpu.make_async_copy(outv.at[pl.ds(*rng)], out.at[pl.ds(*rng)], loc.at[i])
-              for i, rng in enumerate((top, low))]
-    result[0].start()
+    finish(xb1, top, 16, out)
     for hop in last:
         gather_hop(6, hop)
     gather_pair(6, 1)
@@ -602,8 +604,7 @@
     for k in far:
         mix(1, mb1, low, 1, k)
     matmul(1, wo, low, far)
-    finish(xb1, low, 16, outv)
-    result[1].start()
+    finish(xb1, low, 16, out)
 
     ring_drain()
     for g in range(7):
@@ -614,8 +615,6 @@
         for h in range(2):
             stats_all(l, h).wait_send()
     ln_all.wait_send()
-    for c in result:
-        c.wait()
 
 
 def build(mesh, nz, ny, nx):
@@ -633,19 +632,18 @@
         lanes = ((r1 // 2 + BLK - 1) // BLK * BLK + 127) // 128 * 128
         dma, f32, b16 = pltpu.SemaphoreType.DMA, jnp.float32, jnp.bfloat16
         hops = max(nz, ny) // 2
-        anywhere = pl.BlockSpec(memory_space=pl.ANY)
+        outside = pl.BlockSpec(memory_space=pltpu.HBM)
         return pl.pallas_call(
             functools.partial(kernel, nz, ny, nx, tokens, width),
             out_shape=jax.ShapeDtypeStruct((tokens, C), b16),
-            in_specs=[anywhere] * 9,
-            out_specs=anywhere,
+            in_specs=[outside] * 9,
+            out_specs=pl.BlockSpec(memory_space=pltpu.VMEM),
             scratch_shapes=[
                 pltpu.VMEM((2, tp * C), f32),
                 pltpu.VMEM((width, 2, C), f32),
                 pltpu.VMEM((2, C), f32),
                 pltpu.VMEM((2, C), f32),
                 pltpu.VMEM((2, C), f32),
-                pltpu.VMEM((tokens, C), b16),
                 pltpu.VMEM((2, nz, ny, kb, 2 * C), b16),
                 pltpu.VMEM((2, nz, ny, kb, C), b16),
                 pltpu.VMEM((tp, r0, C), b16),
@@ -673,10 +671,12 @@
                 dma((8,)),
             ],
             compiler_params=pltpu.CompilerParams(
-                collective_id=0, has_side_effects=True, vmem_limit_bytes=56 * 1024 * 1024
+                collective_id=0, has_side_effects=True, vmem_limit_bytes=28 * 1024 * 1024
             ),
         )(
+            *[pltpu.with_memory_space_constraint(v, pltpu.HBM) for v in (
             stream, a_w, g_w, o_w, norm_gain, jnp.transpose(conv_w, (1, 0, 2)), conv_b, ln_gain, ln_shift,
+            )]
         )
 
     return jax.shard_map(local, mesh=mesh, in_specs=spec, out_specs=P("sp", "tp"), check_vma=False)

time: 79.6 us -> 75.2 us (0.945)
  Pallas kernels: 77.8 us -> 74.4 us
  local copies, waits for them, and re-layouts: 1.62 us -> 0.68 us
    pallas_call x1, Pallas kernels: 77.8 us -> 74.4 us  [local(): pl.pallas_call(functools.partial(kernel, nz, ny, nx, tokens, width), out_...]
    unnamed x1, local copies, waits for them, and re-layouts: 1.62 us -> 0.68 us
where the time goes in v4:
time: 75.2 us; the launch traced here: 75 us
  Pallas kernels  74.4 us (99%)
    pallas_call x1, Pallas kernels, local(): pl.pallas_call(functools.partial(kernel, nz, ny, nx, tokens, width), out_...  74.4 us

profile of v4, /device:TPU:1, one launch (start us, length us, event | category | flops | bytes accessed | tf_op | source)
XLA Modules:
  0.0 75.0 jit_solution(16375486394295416299)
XLA Ops:
  0.0 74.4 %shard_map.91 = bf16[384,256]{1,0:T(8,128)(2,1)S(1)} custom-call(bf16[384,256]{1,0:T(8,128)(2,1)} %stream.1, bf16[2,32,256]{2,1,0:T(8,128)(2,1)} %a_w.1, bf16[2,32,256]{2,1,0:T(8,128)(2,1)} %g_w.1, bf16[2,32,256]{2,1,0:T(8,128)(2,1)} %o_w.1, f32[2,2048]{1,0:T(2,128)} %norm_gain_in.1, f32[31,2,256]{2,1,0:T(2,128)} %bitcast.1, f32[2,256]{1,0:T(2,128)} %conv_b_in.1, ...), custom_call_target="tpu_custom_call" | custom-call | tf_op jit(solution)/shard_map/pallas_call | solution.py:636
  74.4 0.7 copy.11

commit v5 on v4

--- a/solution.py
+++ b/solution.py
@@ -12,7 +12,7 @@
 C = 256
 HALO = 32
 BLK = 32
-SUB = (4, 2, 4, 1)
+SUB = (4, 2, 2, 1)
 ITEMS = [(st, h) for st in range(4) for h in range(SUB[st])]
 
 
@@ -503,11 +503,11 @@
         mix(0, mb0, top, 0, k)
     ring(1, 3)
     ring(1, 4)
+    for hop in last:
+        gather_hop(2, hop)
     matmul_whole(0, wo, top)
     finish(xb0, top, 16, xb1.at[me])
     gather_start(3)
-    for hop in last:
-        gather_hop(2, hop)
     gather_pair(2, 1)
     for k in near:
         mix(0, mb0, low, 1, k)
@@ -541,20 +541,20 @@
         gather_pair(3, hop)
     for k in far:
         prepare(1, xb1, top, k)
+    factors(top)
+    for hop in last:
+        gather_hop(4, hop)
+    gather_pair(4, 1)
+    for k in near:
+        prepare(1, xb1, low, k)
     ring(2, 3)
     ring(2, 4)
     matmul_whole(1, wag, top)
-    factors(top)
     gate(top, HALO // 2)
     convolve(1, mb1, (0, cut - HALO))
     stats_send(1, 0)
     gather_start(5)
     ring(3, 2)
-    for hop in last:
-        gather_hop(4, hop)
-    gather_pair(4, 1)
-    for k in near:
-        prepare(1, xb1, low, k)
     for hop in last:
         gather_pair(4, hop)
     for k in far:

time: 75.2 us -> 74.9 us (level)
  no operation moved by 1% of the time
where the time goes in v5:
time: 74.9 us; the launch traced here: 74.8 us
  Pallas kernels  74.1 us (99%)
    pallas_call x1, Pallas kernels, local(): pl.pallas_call(functools.partial(kernel, nz, ny, nx, tokens, width), out_...  74.1 us

profile of v5, /device:TPU:1, one launch (start us, length us, event | category | flops | bytes accessed | tf_op | source)
XLA Modules:
  0.0 74.8 jit_solution(15311485727786004118)
XLA Ops:
  0.0 74.1 %shard_map.91 = bf16[384,256]{1,0:T(8,128)(2,1)S(1)} custom-call(bf16[384,256]{1,0:T(8,128)(2,1)} %stream.1, bf16[2,32,256]{2,1,0:T(8,128)(2,1)} %a_w.1, bf16[2,32,256]{2,1,0:T(8,128)(2,1)} %g_w.1, bf16[2,32,256]{2,1,0:T(8,128)(2,1)} %o_w.1, f32[2,2048]{1,0:T(2,128)} %norm_gain_in.1, f32[31,2,256]{2,1,0:T(2,128)} %bitcast.1, f32[2,256]{1,0:T(2,128)} %conv_b_in.1, ...), custom_call_target="tpu_custom_call" | custom-call | tf_op jit(solution)/shard_map/pallas_call | solution.py:636
  74.1 0.7 copy.11

commit v6 on v5

--- a/solution.py
+++ b/solution.py
@@ -12,7 +12,7 @@
 C = 256
 HALO = 32
 BLK = 32
-SUB = (4, 2, 2, 1)
+SUB = (4, 1, 2, 1)
 ITEMS = [(st, h) for st in range(4) for h in range(SUB[st])]
 
 

time: 74.9 us -> 76.3 us (1.019)
  Pallas kernels: 74.1 us -> 75.5 us
    pallas_call x1, Pallas kernels: 74.1 us -> 75.5 us  [local(): pl.pallas_call(functools.partial(kernel, nz, ny, nx, tokens, width), out_...]
where the time goes in v6:
time: 76.3 us; the launch traced here: 76.2 us
  Pallas kernels  75.5 us (99%)
    pallas_call x1, Pallas kernels, local(): pl.pallas_call(functools.partial(kernel, nz, ny, nx, tokens, width), out_...  75.5 us

profile of v6, /device:TPU:1, one launch (start us, length us, event | category | flops | bytes accessed | tf_op | source)
XLA Modules:
  0.0 76.2 jit_solution(5851520378026130152)
XLA Ops:
  0.0 75.5 %shard_map.91 = bf16[384,256]{1,0:T(8,128)(2,1)S(1)} custom-call(bf16[384,256]{1,0:T(8,128)(2,1)} %stream.1, bf16[2,32,256]{2,1,0:T(8,128)(2,1)} %a_w.1, bf16[2,32,256]{2,1,0:T(8,128)(2,1)} %g_w.1, bf16[2,32,256]{2,1,0:T(8,128)(2,1)} %o_w.1, f32[2,2048]{1,0:T(2,128)} %norm_gain_in.1, f32[31,2,256]{2,1,0:T(2,128)} %bitcast.1, f32[2,256]{1,0:T(2,128)} %conv_b_in.1, ...), custom_call_target="tpu_custom_call" | custom-call | tf_op jit(solution)/shard_map/pallas_call | solution.py:636
  75.5 0.7 copy.11
